TPU v7x, 32 devices: a whole 2x2x4 slice. The times are simulated.
32 devices in a mesh: sp: 4 (over y, x), tp: 8 (over z, core).
Axes of the slice: x: 2, y: 2, z: 4, core: 2. Of those that a mesh axis runs over, the one named last changes fastest.
Arguments:
- latent: bfloat16 [4096, 2048], P(('sp', 'tp')), may hold values from -1.5 to 1.5
- context: bfloat16 [128, 2048], P('sp'), may hold values from -6 to 6
- cond: bfloat16 [2048], replicated, may hold values from -6 to 6
- cond_context: bfloat16 [2048], replicated, may hold values from -6 to 6
- mod_weight: bfloat16 [3, 2048, 2048], P(None, 'sp', 'tp'), may hold values from -0.125 to 0.125
- norm_gain: bfloat16 [2048], replicated, may hold values from 0.099609375 to 1.8984375
- down_q: bfloat16 [2048, 768], P('tp'), may hold values from -0.125 to 0.125
- down_kv: bfloat16 [2048, 512], P('tp'), may hold values from -0.125 to 0.125
- rope_weight: bfloat16 [2048, 32], replicated, may hold values from -0.125 to 0.125
- qlat_gain: bfloat16 [768], replicated, may hold values from 0.099609375 to 1.8984375
- kvlat_gain: bfloat16 [512], replicated, may hold values from 0.099609375 to 1.8984375
- up_query: bfloat16 [768, 1536], P(None, 'tp'), may hold values from -0.21875 to 0.21875
- up_key: bfloat16 [512, 1024], P(None, 'tp'), may hold values from -0.25 to 0.25
- up_value: bfloat16 [512, 1024], P(None, 'tp'), may hold values from -0.25 to 0.25
- query_gain: float32 [96], replicated, may hold values from 0.5 to 8
- key_gain: float32 [96], replicated, may hold values from 0.5 to 8
- context_bias: float32 [16], P('tp'), may hold values from -2.2 to -0.7
- out_weight: bfloat16 [1024, 2048], P('tp'), may hold values from -24 to 24
Outputs:
- mixed: bfloat16 [4096, 2048], P(('sp', 'tp'))
All inputs are finite; a program needn't handle non-finite values.
Results may differ from a plain program's by a relative error of at most 0.028.
The roundings to bfloat16 on the way count: a program that leaves them out, or rounds other values in their place, can miss the bound.
Values may be sent and summed in bfloat16 or wider, within the bound.
A program may use at most 64 MiB of HBM per device.

v0:
```python
import math

import jax
import jax.numpy as jnp
from jax import lax
from jax.experimental import pallas as pl
from jax.experimental.pallas import tpu as pltpu
from jax.sharding import PartitionSpec as P

NOPE = 64
ROPE = 32
VDIM = 64
GRID_W = 64
TOK_DEV = 1024
CTX_DEV = 32


epsilon = 1e-06
theta = 10000.0


def rms_scale(tensor, gain):
    return (
        tensor
        * lax.rsqrt(jnp.mean(tensor * tensor, axis=-1, keepdims=True) + epsilon)
        * gain.astype(jnp.float32)
    )


def axial_tables(positions):
    pair_count = ROPE // 4
    frequency = jnp.power(theta, -jnp.arange(pair_count, dtype=jnp.float32) / pair_count)
    row_angle = (positions // GRID_W).astype(jnp.float32)[:, None] * frequency
    col_angle = (positions % GRID_W).astype(jnp.float32)[:, None] * frequency
    return (jnp.cos(row_angle), jnp.sin(row_angle), jnp.cos(col_angle), jnp.sin(col_angle))


def rotate_half(tensor, cosine, sine_table):
    first, second = jnp.split(tensor, 2, axis=-1)
    cosine = cosine[:, None, :]
    sine_table = sine_table[:, None, :]
    return jnp.concatenate(
        [first * cosine - second * sine_table, second * cosine + first * sine_table], axis=-1
    )


def axial_rotate(tensor, tables):
    half_width = tensor.shape[-1] // 2
    return jnp.concatenate(
        [
            rotate_half(tensor[..., :half_width], tables[0], tables[1]),
            rotate_half(tensor[..., half_width:], tables[2], tables[3]),
        ],
        axis=-1,
    )


def modulate(row_block, gain, shifts, scales):
    normal = rms_scale(row_block.astype(jnp.float32), gain)
    return (normal * (1.0 + scales) + shifts).astype(jnp.bfloat16)


def make_queries(query_latent, up_query, query_gain, tables):
    amount = query_latent.shape[0]
    projected = jnp.dot(query_latent, up_query, preferred_element_type=jnp.float32).reshape(
        amount, -1, NOPE + ROPE
    )
    normal = rms_scale(projected, query_gain)
    return jnp.concatenate(
        [normal[..., :NOPE], axial_rotate(normal[..., NOPE:], tables)], axis=-1
    ).astype(jnp.bfloat16)


def make_keys(kv_latent, rope_rows, up_key, up_value, key_gain, tables):
    amount = kv_latent.shape[0]
    unrotated = jnp.dot(kv_latent, up_key, preferred_element_type=jnp.float32).reshape(
        amount, -1, NOPE
    )
    head_count = unrotated.shape[1]
    shared = jnp.broadcast_to(rope_rows.astype(jnp.float32)[:, None, :], (amount, head_count, ROPE))
    normal = rms_scale(jnp.concatenate([unrotated, shared], axis=-1), key_gain)
    if tables is not None:
        normal = jnp.concatenate(
            [normal[..., :NOPE], axial_rotate(normal[..., NOPE:], tables)], axis=-1
        )
    values = jnp.dot(kv_latent, up_value, preferred_element_type=jnp.float32).reshape(
        amount, head_count, VDIM
    )
    return (normal.astype(jnp.bfloat16), values.astype(jnp.bfloat16))


CORES = 2


def greet(sp_peers=True):
    sp, tp = lax.axis_index("sp"), lax.axis_index("tp")
    S, T = lax.axis_size("sp"), lax.axis_size("tp")
    barrier = pltpu.get_barrier_semaphore()
    for k in range(1, S):
        pl.semaphore_signal(barrier, inc=1, device_id={"sp": lax.rem(sp + k, S)}, device_id_type=pl.DeviceIdType.MESH)
    for k in range(1, T):
        pl.semaphore_signal(barrier, inc=1, device_id={"tp": lax.rem(tp + k, T)}, device_id_type=pl.DeviceIdType.MESH)
    pl.semaphore_wait(barrier, S + T - 2)


def remote(source, target, send, recv, device):
    return pltpu.make_async_remote_copy(
        src_ref=source,
        dst_ref=target,
        send_sem=send,
        recv_sem=recv,
        device_id=device,
        device_id_type=pl.DeviceIdType.MESH,
    )


class Line:
    def __init__(self, own, slots, send, recv, z, core, Z):
        self.own, self.slots, self.send, self.recv = own, slots, send, recv
        self.z, self.core, self.Z = z, core, Z

    def hop(self, block, step, first=False):
        to = lax.max(lax.min(self.z + step, self.Z - 1), 0)
        d = 0 if step > 0 else 1
        return remote(
            self.own if first else self.slots(block),
            self.slots(block),
            self.send.at[block, d],
            self.recv.at[block],
            {"tp": to * CORES + self.core},
        )

    def start(self):
        for step in (1, -1):
            ok = (self.z + step >= 0) & (self.z + step < self.Z)

            @pl.when(ok)
            def _():
                self.hop(self.z, step, True).start()

    def each(self, body):
        for k in range(1, self.Z):
            for step in (1, -1):
                block = self.z - step * k

                @pl.when((block >= 0) & (block < self.Z))
                def _():
                    body(block, step)

    def arrive(self, block, step):
        self.hop(block, step).wait_recv()
        ok = (self.z + step >= 0) & (self.z + step < self.Z)

        @pl.when(ok)
        def _():
            self.hop(block, step).start()

    def drain(self):
        for step in (1, -1):
            ok = (self.z + step >= 0) & (self.z + step < self.Z)

            @pl.when(ok)
            def _():
                self.hop(self.z, step, True).wait_send()

        def body(block, step):
            ok = (self.z + step >= 0) & (self.z + step < self.Z)

            @pl.when(ok)
            def _():
                self.hop(block, step).wait_send()

        self.each(body)


def loop(low, high, body):
    def step(k, carry):
        body(k)
        return carry

    lax.fori_loop(low, high, step, 0)


def weights_kernel(
    act, mod_weight, dq, dkv, ow, mods, dq_all, dkv_all, ow_part,
    pm, msum, m_send, m_recv, t_send, t_recv, l_send, l_recv, s_send, s_recv, c_send, c_recv, loc,
):
    sp, tp = lax.axis_index("sp"), lax.axis_index("tp")
    S, T = lax.axis_size("sp"), lax.axis_size("tp")
    Z = T // CORES
    z, core = tp // CORES, lax.rem(tp, CORES)
    mate = {"tp": tp + 1 - 2 * core}
    for r in range(mod_weight.shape[0]):
        pm[sp, r * 8 : (r + 1) * 8, :] = jnp.dot(act[...], mod_weight[r], preferred_element_type=jnp.float32)
    greet()
    downs = ((dq, dq_all), (dkv, dkv_all))

    def part_copy(k):
        return remote(pm.at[sp], pm.at[sp], m_send.at[k], m_recv.at[k], {"sp": lax.rem(sp + k, S)})

    lines = [
        Line(a.at[sp], (lambda o: lambda b: o.at[b, core, sp])(o), l_send.at[i], l_recv.at[i], z, core, Z)
        for i, (a, o) in enumerate(downs)
    ]
    lines.append(Line(ow.at[sp], lambda b: ow_part.at[b], l_send.at[2], l_recv.at[2], z, core, Z))
    for line in lines[:2]:
        line.start()
    loop(1, S, lambda k: part_copy(k).start())
    local = []
    for i, (a, o) in enumerate(downs):
        local.append(pltpu.make_async_copy(a, o.at[z, core], loc.at[i]))
    local.append(pltpu.make_async_copy(ow.at[sp], ow_part.at[z], loc.at[2]))
    for copy in local:
        copy.start()

    def mate_copy(i, block, own=False):
        a, o = downs[i]
        return remote(
            a if own else o.at[block, core], o.at[block, core], c_send.at[i, block], c_recv.at[i, block], mate
        )

    def mate_wait(i, block):
        a, o = downs[i]
        to = o.at[block, 1 - core]
        remote(to, to, c_send.at[i, block], c_recv.at[i, block], mate).wait_recv()

    for i in range(2):
        mate_copy(i, z, True).start()

    def part_wait(k):
        to = pm.at[lax.rem(sp - k + S, S)]
        remote(to, to, m_send.at[k], m_recv.at[k], {"sp": lax.rem(sp + k, S)}).wait_recv()

    loop(1, S, part_wait)
    total = pm[0]
    for k in range(1, S):
        total = total + pm[k]
    msum[...] = total
    mods[tp] = total

    def spread(i, block, k):
        at = downs[i][1].at[block, core, sp]
        return remote(at, at, s_send.at[i, block, k], s_recv.at[i, block, k], {"sp": lax.rem(sp + k, S)})

    def gathered(i, block, k):
        at = downs[i][1].at[block, core, lax.rem(sp - k + S, S)]
        return remote(at, at, s_send.at[i, block, k], s_recv.at[i, block, k], {"sp": lax.rem(sp + k, S)})

    def body(block, step):
        for i in range(2):
            lines[i].arrive(block, step)
            loop(1, S, lambda k: spread(i, block, k).start())

    def mod_copy(k):
        return remote(msum, mods.at[tp], t_send.at[k], t_recv.at[k], {"tp": lax.rem(tp + k, T)})

    def mod_wait(k):
        to = mods.at[lax.rem(tp - k + T, T)]
        remote(msum, to, t_send.at[k], t_recv.at[k], {"tp": lax.rem(tp + k, T)}).wait_recv()

    loop(1, T, lambda k: mod_copy(k).start())
    lines[0].each(body)
    lines[2].start()
    lines[2].each(lines[2].arrive)

    def body(block, step):
        for i in range(2):
            loop(1, S, lambda k: gathered(i, block, k).wait_recv())
            mate_copy(i, block).start()

    lines[0].each(body)
    for copy in local:
        copy.wait()
    loop(1, T, mod_wait)
    for i in range(2):
        for b in range(Z):
            mate_wait(i, b)
    for i in range(2):
        mate_copy(i, z, True).wait_send()

    def body(block, step):
        for i in range(2):
            mate_copy(i, block).wait_send()
            loop(1, S, lambda k: spread(i, block, k).wait_send())

    lines[0].each(body)
    for line in lines:
        line.drain()
    loop(1, S, lambda k: part_copy(k).wait_send())
    loop(1, T, lambda k: mod_copy(k).wait_send())


def attend_kernel(
    lat_kv, lat_q, ow_part, ctx, shift, uq, ukv, pick, gain_q, gain_k, tables,
    out, ow_all,
    kv_lats, q_lats, q, kv, kv_all, ctx_all, m_scr, l_scr, acc, att,
    l_send, l_recv, c_send, c_recv, s_send, s_recv,
    k_send, k_recv, x_send, x_recv, a_send, a_recv, loc,
):
    sp, tp = lax.axis_index("sp"), lax.axis_index("tp")
    S, T = lax.axis_size("sp"), lax.axis_size("tp")
    Z = T // CORES
    z, core = tp // CORES, lax.rem(tp, CORES)
    mate = {"tp": tp + 1 - 2 * core}
    H, N, _ = q.shape
    rows = out.shape[1]
    span = rows * CORES
    KD = NOPE + ROPE
    TQ = math.gcd(N, 256)
    WIDE = KD + VDIM
    factor = KD ** (-0.5) * math.log2(math.e)
    greet()
    lats = ((lat_kv, kv_lats), (lat_q, q_lats))
    lines = [
        Line(own, (lambda o: lambda b: o.at[b, core])(every), l_send.at[i], l_recv.at[i], z, core, Z)
        for i, (own, every) in enumerate(lats)
    ]

    def mate_copy(i, block, own=False):
        to = lats[i][1].at[block, core]
        return remote(lats[i][0] if own else to, to, c_send.at[i, block], c_recv.at[i, block], mate)

    def mate_wait(i, block):
        to = lats[i][1].at[block, 1 - core]
        remote(to, to, c_send.at[i, block], c_recv.at[i, block], mate).wait_recv()

    lines[0].start()
    mate_copy(0, z, True).start()
    lines[1].start()
    mate_copy(1, z, True).start()

    def ctx_copy(k):
        return remote(ctx, ctx_all.at[sp], x_send.at[k], x_recv.at[k], {"sp": lax.rem(sp + k, S)})

    def ctx_wait(k):
        to = ctx_all.at[lax.rem(sp - k + S, S)]
        remote(ctx, to, x_send.at[k], x_recv.at[k], {"sp": lax.rem(sp + k, S)}).wait_recv()

    def kv_copy(k):
        return remote(kv, kv_all.at[sp], k_send.at[k], k_recv.at[k], {"sp": lax.rem(sp + k, S)})

    def spread(k):
        return remote(ow_part, ow_all.at[:, core, sp], s_send.at[k], s_recv.at[k], {"sp": lax.rem(sp + k, S)})

    def gathered(k):
        to = ow_all.at[:, core, lax.rem(sp - k + S, S)]
        return remote(ow_part, to, s_send.at[k], s_recv.at[k], {"sp": lax.rem(sp + k, S)})

    loop(1, S, lambda k: ctx_copy(k).start())
    loop(1, S, lambda k: spread(k).start())
    own_ow = pltpu.make_async_copy(ow_part, ow_all.at[:, core, sp], loc)
    own_ow.start()
    ctx_all[sp] = ctx[...]
    kv_lats[z, core] = lat_kv[...]
    q_lats[z, core] = lat_q[...]

    NT = (((1,), (1,)), ((), ()))

    def turned(u, gain, at):
        u = u * lax.rsqrt(jnp.mean(u * u, axis=0, keepdims=True) + epsilon) * gain[:, :1]
        m = ROPE // 4
        a, b, c, d = (u[NOPE + i * m : NOPE + (i + 1) * m, :] for i in range(4))
        rc, rs, cc, cs = (tables[i, :, at] for i in range(4))
        return jnp.concatenate(
            [u[:NOPE, :], a * rc - b * rs, b * rc + a * rs, c * cc - d * cs, d * cc + c * cs], axis=0
        )

    def passed(i):
        def body(block, step):
            lines[i].arrive(block, step)
            mate_copy(i, block).start()

        lines[i].each(body)

    passed(0)
    rank = ukv.shape[1]

    def expand_kv(b):
        mate_wait(0, b)
        at = pl.ds(pl.multiple_of(b * span, span), span)
        rows_in = kv_lats[b].reshape(span, kv_lats.shape[3])
        u = lax.dot_general(ukv[...], rows_in[:, :rank], NT, preferred_element_type=jnp.float32)
        rope = lax.dot_general(pick[...], rows_in[:, rank:], NT, preferred_element_type=jnp.float32)
        for h in range(H):
            key = turned(jnp.concatenate([u[h * NOPE : (h + 1) * NOPE, :], rope], axis=0), gain_k[...], at)
            kv[h * WIDE : h * WIDE + KD, at] = key.astype(jnp.bfloat16)
            base = H * NOPE + h * VDIM
            kv[h * WIDE + KD : (h + 1) * WIDE, at] = u[base : base + VDIM, :].astype(jnp.bfloat16)

    loop(0, Z, expand_kv)
    loop(1, S, lambda k: kv_copy(k).start())
    passed(1)

    def expand_q(b):
        mate_wait(1, b)
        at = pl.ds(pl.multiple_of(b * span, span), span)
        rows_in = q_lats[b].reshape(span, q_lats.shape[3])
        u = lax.dot_general(uq[...], rows_in, NT, preferred_element_type=jnp.float32)
        for h in range(H):
            query = turned(u[h * KD : (h + 1) * KD, :], gain_q[...], at)
            query = jnp.concatenate([query, jnp.zeros((128 - KD, span), jnp.float32)], axis=0)
            q[h, at, :] = query.T.astype(jnp.bfloat16)

    loop(0, Z, expand_q)

    def lanes(p):
        total = p[:, :128]
        for j in range(1, p.shape[1] // 128):
            total = total + p[:, j * 128 : (j + 1) * 128]
        return total

    def first(qi):
        at = pl.ds(pl.multiple_of(qi * TQ, TQ), TQ)
        for h in range(H):
            kt = kv[h * WIDE : h * WIDE + KD, :]
            vt = kv[h * WIDE + KD : (h + 1) * WIDE, :]
            s = jnp.dot(q[h, at, :][:, :KD], kt, preferred_element_type=jnp.float32) * factor
            new = jnp.max(s, axis=1, keepdims=True)
            p = jnp.exp2(s - new)
            m_scr[h, at, :] = jnp.broadcast_to(new, (TQ, 128))
            l_scr[h, at, :] = lanes(p)
            acc[h, at, :] = lax.dot_general(p.astype(jnp.bfloat16), vt, NT, preferred_element_type=jnp.float32)

    loop(0, N // TQ, first)

    def absorb(h, at, s, value, dims):
        old = m_scr[h, at, :][:, :1]
        new = jnp.maximum(old, jnp.max(s, axis=1, keepdims=True))
        scale = jnp.exp2(old - new)
        p = jnp.exp2(s - new)
        m_scr[h, at, :] = jnp.broadcast_to(new, (TQ, 128))
        l_scr[h, at, :] = l_scr[h, at, :] * scale + lanes(p)
        acc[h, at, :] = acc[h, at, :] * scale + lax.dot_general(
            p.astype(jnp.bfloat16), value, (dims, ((), ())), preferred_element_type=jnp.float32
        )

    loop(1, S, ctx_wait)

    def context_step(qi):
        at = pl.ds(pl.multiple_of(qi * TQ, TQ), TQ)
        for h in range(H):
            rows_all = ctx_all[...].reshape(-1, ctx_all.shape[2])
            kc = rows_all[:, h * 256 : h * 256 + 128][:, :KD]
            vc = rows_all[:, h * 256 + 128 : h * 256 + 256][:, :VDIM]
            s = lax.dot_general(q[h, at, :][:, :KD], kc, (((1,), (1,)), ((), ())), preferred_element_type=jnp.float32)
            s = s * factor + shift[h : h + 1, :1]
            absorb(h, at, s, vc, ((1,), (0,)))

    loop(0, N // TQ, context_step)

    def latent_step(k):
        slot = lax.rem(sp - k + S, S)
        to = kv_all.at[slot]
        remote(kv, to, k_send.at[k], k_recv.at[k], {"sp": lax.rem(sp + k, S)}).wait_recv()

        def tile(qi):
            at = pl.ds(pl.multiple_of(qi * TQ, TQ), TQ)
            for h in range(H):
                kt = kv_all[slot, h * WIDE : h * WIDE + KD, :]
                vt = kv_all[slot, h * WIDE + KD : (h + 1) * WIDE, :]
                s = jnp.dot(q[h, at, :][:, :KD], kt, preferred_element_type=jnp.float32) * factor
                absorb(h, at, s, vt, ((1,), (1,)))

        loop(0, N // TQ, tile)

    own_ow.wait()
    loop(1, S, lambda k: gathered(k).wait_recv())
    half = ow_all.at[:, core]
    whole = remote(half, half, c_send.at[0, Z], c_recv.at[0, Z], mate)
    whole.start()
    loop(1, S, latent_step)

    def finish(qi):
        at = pl.ds(pl.multiple_of(qi * TQ, TQ), TQ)
        heads = [acc[h, at, :] / jnp.sum(l_scr[h, at, :], axis=1, keepdims=True) for h in range(H)]
        att[at, :] = jnp.concatenate(heads, axis=1).astype(jnp.bfloat16)

    loop(0, N // TQ, finish)

    def give(k):
        peer = lax.rem(tp + k, T)
        return remote(
            att.at[pl.ds(pl.multiple_of(peer * rows, rows), rows)], out.at[tp], a_send.at[k], a_recv.at[k], {"tp": peer}
        )

    def take(k):
        to = out.at[lax.rem(tp - k + T, T)]
        remote(to, to, a_send.at[k], a_recv.at[k], {"tp": lax.rem(tp + k, T)}).wait_recv()

    loop(1, T, lambda k: give(k).start())
    out[tp] = att[pl.ds(pl.multiple_of(tp * rows, rows), rows), :]
    loop(1, T, take)
    loop(1, T, lambda k: give(k).wait_send())
    loop(1, S, lambda k: kv_copy(k).wait_send())
    loop(1, S, lambda k: ctx_copy(k).wait_send())
    loop(1, S, lambda k: spread(k).wait_send())
    to = ow_all.at[:, 1 - core]
    remote(to, to, c_send.at[0, Z], c_recv.at[0, Z], mate).wait_recv()
    whole.wait_send()
    for i in range(2):
        mate_copy(i, z, True).wait_send()
        lines[i].each(lambda block, step: mate_copy(i, block).wait_send())
        lines[i].drain()


DMA = pltpu.SemaphoreType.DMA
VM = pl.BlockSpec(memory_space=pltpu.VMEM)
ANY = pl.BlockSpec(memory_space=pl.ANY)


def call(kernel, ident, outs, out_specs, scratch, args):
    return pl.pallas_call(
        kernel,
        out_shape=outs,
        in_specs=[VM] * len(args),
        out_specs=out_specs,
        scratch_shapes=scratch,
        compiler_params=pltpu.CompilerParams(
            collective_id=ident, has_side_effects=True, vmem_limit_bytes=48 * 1024 * 1024
        ),
    )(*args)


def shards(
    latent, context, cond, cond_context, mod_weight, norm_gain, down_q, down_kv, rope_weight, qlat_gain, kvlat_gain,
    up_query, up_key, up_value, query_gain, key_gain, context_bias, out_weight,
):
    seq_index = lax.axis_index("sp")
    S, T = lax.axis_size("sp"), lax.axis_size("tp")
    Z = T // CORES
    bf16, f32 = jnp.bfloat16, jnp.float32
    own_rows = latent.shape[0]
    block_tokens = own_rows * T
    row_span, cols = mod_weight.shape[1:]
    width = latent.shape[1]
    activated = jax.nn.silu(jnp.stack([cond, cond_context]).astype(f32)).astype(bf16)
    own_part = lax.dynamic_slice_in_dim(activated, seq_index * row_span, row_span, 1)
    act = jnp.concatenate([own_part, jnp.zeros((6, row_span), bf16)], axis=0)
    pieces = [w.reshape(S, w.shape[0] // S, w.shape[1]) for w in (down_q, down_kv, out_weight)]
    dq, dkv, ow = pieces
    mods, dq_all, dkv_all, ow_part = call(
        weights_kernel,
        1,
        (
            jax.ShapeDtypeStruct((T, 24, cols), f32),
            jax.ShapeDtypeStruct((Z, CORES) + dq.shape, bf16),
            jax.ShapeDtypeStruct((Z, CORES) + dkv.shape, bf16),
            jax.ShapeDtypeStruct((Z,) + ow.shape[1:], bf16),
        ),
        (VM, ANY, ANY, ANY),
        [
            pltpu.VMEM((S, 24, cols), f32), pltpu.VMEM((24, cols), f32),
            DMA((S,)), DMA((S,)), DMA((T,)), DMA((T,)),
            DMA((3, Z, 2)), DMA((3, Z)), DMA((2, Z, S)), DMA((2, Z, S)), DMA((2, Z)), DMA((2, Z)), DMA((3,)),
        ],
        (act, mod_weight, dq, dkv, ow),
    )
    mods = mods.transpose(1, 0, 2).reshape(24, width)
    normed = modulate(latent, norm_gain, mods[0], mods[8])
    context_normed = modulate(context, norm_gain, mods[1], mods[9])
    gates = mods[16]
    stacked = jnp.concatenate([normed, context_normed], axis=0)
    query_down = jnp.dot(normed, dq_all.reshape(width, -1), preferred_element_type=f32)
    kv_down = jnp.dot(stacked, dkv_all.reshape(width, -1), preferred_element_type=f32)
    query_latent = rms_scale(query_down, qlat_gain).astype(bf16)
    kv_latent = rms_scale(kv_down, kvlat_gain).astype(bf16)
    rope_rows = jnp.dot(stacked, rope_weight, preferred_element_type=f32).astype(bf16)
    QR, KR = query_latent.shape[1], kv_latent.shape[1]
    lat_kv = jnp.concatenate(
        [kv_latent[:own_rows], jnp.pad(rope_rows[:own_rows], ((0, 0), (0, 128 - ROPE)))], axis=1
    )
    ctx_keys, ctx_values = make_keys(
        kv_latent[own_rows:], rope_rows[own_rows:], up_key, up_value, key_gain, None
    )
    H = ctx_keys.shape[1]
    KD = NOPE + ROPE
    ctx = jnp.concatenate(
        [jnp.pad(ctx_keys, ((0, 0), (0, 0), (0, 128 - KD))), jnp.pad(ctx_values, ((0, 0), (0, 0), (0, 128 - VDIM)))],
        axis=-1,
    ).reshape(-1, H * 256)
    positions = seq_index * block_tokens + jnp.arange(block_tokens, dtype=jnp.int32)
    tables = axial_tables(positions)
    tables = jnp.stack([table.T for table in tables])
    uq = up_query.T
    ukv = jnp.concatenate([up_key, up_value], axis=1).T
    pick = jnp.eye(ROPE, 128, dtype=bf16)
    gain_q = jnp.broadcast_to(query_gain[:, None], (KD, 128))
    gain_k = jnp.broadcast_to(key_gain[:, None], (KD, 128))
    shift = (context_bias + math.log(TOK_DEV / CTX_DEV)) * math.log2(math.e)
    shift = jnp.broadcast_to(shift[:, None], (H, 128))
    kv_rows = H * (KD + VDIM)
    token_rows, ow_all = call(
        attend_kernel,
        2,
        (
            jax.ShapeDtypeStruct((T, own_rows, H * VDIM), bf16),
            jax.ShapeDtypeStruct((Z, CORES) + ow.shape, bf16),
        ),
        (VM, ANY),
        [
            pltpu.VMEM((Z, CORES) + lat_kv.shape, bf16), pltpu.VMEM((Z, CORES) + query_latent.shape, bf16),
            pltpu.VMEM((H, block_tokens, 128), bf16), pltpu.VMEM((kv_rows, block_tokens), bf16),
            pltpu.VMEM((S, kv_rows, block_tokens), bf16), pltpu.VMEM((S,) + ctx.shape, bf16),
            pltpu.VMEM((H, block_tokens, 128), f32), pltpu.VMEM((H, block_tokens, 128), f32),
            pltpu.VMEM((H, block_tokens, VDIM), f32), pltpu.VMEM((block_tokens, H * VDIM), bf16),
            DMA((2, Z, 2)), DMA((2, Z)), DMA((2, Z + 1)), DMA((2, Z + 1)), DMA((S,)), DMA((S,)),
            DMA((S,)), DMA((S,)), DMA((S,)), DMA((S,)), DMA((T,)), DMA((T,)), DMA,
        ],
        (lat_kv, query_latent, ow_part, ctx, shift, uq, ukv, pick, gain_q, gain_k, tables),
    )
    token_rows = token_rows.transpose(1, 0, 2).reshape(own_rows, -1)
    projected = jnp.dot(token_rows, ow_all.reshape(-1, width), preferred_element_type=f32)
    return (latent.astype(f32) + gates * projected).astype(bf16)


def solution(mesh):
    in_specs = (
        P(("sp", "tp"), None),
        P("sp", None),
        P(),
        P(),
        P(None, "sp", "tp"),
        P(),
        P("tp", None),
        P("tp", None),
        P(),
        P(),
        P(),
        P(None, "tp"),
        P(None, "tp"),
        P(None, "tp"),
        P(),
        P(),
        P("tp"),
        P("tp", None),
    )
    out_specs = P(("sp", "tp"), None)
    return jax.shard_map(shards, mesh=mesh, in_specs=in_specs, out_specs=out_specs, check_vma=False)
```

profile of v0, /device:TPU:0, one launch (start us, length us, event | category | flops | bytes accessed | tf_op | source)
XLA Modules:
  0.0 133.5 jit_solution(8170605095823139234)
XLA Ops:
  0.0 0.7 stack.16
  0.7 0.7 stack.17
  1.5 1.1 copy-done.2
  2.6 1.0 copy-done.3
  3.7 1.0 copy-done.4
  4.7 0.9 copy-done.6
  5.6 39.7 %shard_map.172 = (f32[8,24,256]{2,1,0:T(8,128)S(1)}, bf16[4,2,4,64,768]{4,3,2,1,0:T(8,128)(2,1)}, bf16[4,2,4,64,512]{4,3,2,1,0:T(8,128)(2,1)S(1)}, bf16[4,32,2048]{2,1,0:T(8,128)(2,1)S(1)}) custom-call(bf16[8,512]{1,0:T(8,128)(2,1)S(1)} %concatenate.18.act, bf16[3,512,256]{2,1,0:T(8,128)(2,1)S(1)} %copy-done.2, bf16[4,64,768]{2,1,0:T(8,128)(2,1)S(1)} %bitcast.29, ...), custom_call_target="tpu_custom_call" | custom-call | tf_op jit(solution)/shard_map/pallas_call | solution.py:512
  45.4 0.2 fusion.2
  45.6 0.3 fusion.6
  45.9 0.1 fusion.9
  46.0 0.1 fusion.13
  46.2 0.6 multiply_reduce_fusion.1
  46.8 0.1 multiply_convert_fusion.1
  46.9 0.1 fusion.17
  47.1 0.1 reshape.321
  47.2 0.3 convolution_convert_fusion
  47.5 0.2 multiply_reduce_fusion.2
  47.8 0.1 multiply_convert_fusion.2
  47.9 0.1 convolution_convert_fusion.1
  48.1 0.1 convert_element_type.91
  48.3 2.6 %multiply_reduce_fusion = (f32[128]{0:T(128)S(1)}, f32[128,768]{1,0:T(8,128)S(1)}) fusion(bf16[128,2048]{1,0:T(8,128)(2,1)S(1)} %fusion.6, bf16[2048,768]{1,0:T(8,128)(2,1)} %bitcast.36), kind=kOutput, calls=%fused_computation.15 | convolution fusion | flops 402849664 | bytes 4063744 | tf_op jit(solution)/shard_map/dot_general | solution.py:563
  50.9 0.1 multiply_convert_fusion.lat_q
  51.0 0.3 multiply_cosine_fusion.1
  51.4 0.1 copy.23
  51.5 0.1 copy.24
  51.7 0.1 broadcast_in_dim.10.gain_q
  51.7 0.1 broadcast_in_dim.11.gain_k
  51.8 0.1 broadcast_in_dim.9.shift
  51.9 75.7 %shard_map.173 = (bf16[8,128,128]{2,1,0:T(8,128)(2,1)S(1)}, bf16[4,2,4,32,2048]{4,3,2,1,0:T(8,128)(2,1)S(1)}) custom-call(bf16[128,640]{1,0:T(8,128)(2,1)S(1)} %fusion.14.lat_kv, bf16[128,768]{1,0:T(8,128)(2,1)S(1)} %multiply_convert_fusion.lat_q, bf16[4,32,2048]{2,1,0:T(8,128)(2,1)S(1)} %get-tuple-element.14.ow_part, bf16[32,512]{1,0:T(8,128)(2,1)S(1)} %bitcast.33, ...), custom_call_target="tpu_custom_call" | custom-call | tf_op jit(solution)/shard_map/pallas_call | solution.py:512
  127.6 1.9 %copy-done.1 = bf16[4,2,4,32,2048]{4,3,2,1,0:T(8,128)(2,1)} copy-done((bf16[4,2,4,32,2048]{4,3,2,1,0:T(8,128)(2,1)}, bf16[4,2,4,32,2048]{4,3,2,1,0:T(8,128)(2,1)S(1)}, u32[]{:S(2)}) %copy-start.1) | copy-done | bytes 4194328
  129.6 0.2 copy.25
  129.7 3.7 %fusion.1 = bf16[128,2048]{1,0:T(8,128)(2,1)} fusion(bf16[128,1024]{0,1:T(8,128)(2,1)S(1)} %bitcast.37, bf16[1024,2048]{1,0:T(8,128)(2,1)} %bitcast.27, bf16[128,2048]{1,0:T(8,128)(2,1)S(1)} %copy-done.7, f32[2048]{0:T(1024)S(1)} %bitcast.39), kind=kOutput, calls=%fused_computation.2 | convolution fusion | flops 537919488 | bytes 5513216 | tf_op jit(solution)/shard_map/dot_general | solution.py:612
  (54 shorter events, 0.4 us)
Async XLA Ops:
  0.0 47.2 %copy-start = (bf16[2048,32]{0,1:T(8,128)(2,1)S(1)}, bf16[2048,32]{0,1:T(8,128)(2,1)}, u32[]{:S(2)}) copy-start(bf16[2048,32]{0,1:T(8,128)(2,1)} %param.26) | copy-start | bytes 393220
  0.0 45.3 %copy-start.11 = (bf16[2048]{0:T(1024)(128)(2,1)S(1)}, bf16[2048]{0:T(1024)(128)(2,1)}, u32[]{:S(2)}) copy-start(bf16[2048]{0:T(1024)(128)(2,1)} %param.23) | copy-start | bytes 12292
  1.5 1.1 copy-start.2
  2.6 1.0 copy-start.3
  3.7 1.0 copy-start.4
  4.7 0.9 copy-start.6
  5.6 39.7 %copy-start.7 = (bf16[128,2048]{1,0:T(8,128)(2,1)S(1)}, bf16[128,2048]{1,0:T(8,128)(2,1)}, u32[]{:S(2)}) copy-start(bf16[128,2048]{1,0:T(8,128)(2,1)} %param.18) | copy-start | bytes 1572868
  5.6 40.2 %copy-start.8 = (bf16[32,2048]{1,0:T(8,128)(2,1)S(1)}, bf16[32,2048]{1,0:T(8,128)(2,1)}, u32[]{:S(2)}) copy-start(bf16[32,2048]{1,0:T(8,128)(2,1)} %param.19) | copy-start | bytes 393220
  45.9 1.0 copy-start.14
  46.0 0.9 copy-start.9
  46.2 1.6 %copy-start.12 = (f32[96]{0:T(128)S(1)}, f32[96]{0:T(128)}, u32[]{:S(2)}) copy-start(f32[96]{0:T(128)} %param.33) | copy-start | bytes 1156
  46.2 1.7 %copy-start.10 = (bf16[512,128]{1,0:T(8,128)(2,1)S(1)}, bf16[512,128]{1,0:T(8,128)(2,1)}, u32[]{:S(2)}) copy-start(bf16[512,128]{1,0:T(8,128)(2,1)} %param.31) | copy-start | bytes 393220
  48.3 2.6 %copy-start.13 = (bf16[768]{0:T(1024)(128)(2,1)S(1)}, bf16[768]{0:T(1024)(128)(2,1)}, u32[]{:S(2)}) copy-start(bf16[768]{0:T(1024)(128)(2,1)} %param.27) | copy-start | bytes 4612
  48.3 3.4 %copy-start.15 = (f32[96]{0:T(128)S(1)}, f32[96]{0:T(128)}, u32[]{:S(2)}) copy-start(f32[96]{0:T(128)} %param.32) | copy-start | bytes 1156
  50.8 1.0 copy-start.16
  50.9 1.1 copy-start.5
  127.6 1.9 %copy-start.1 = (bf16[4,2,4,32,2048]{4,3,2,1,0:T(8,128)(2,1)}, bf16[4,2,4,32,2048]{4,3,2,1,0:T(8,128)(2,1)S(1)}, u32[]{:S(2)}) copy-start(bf16[4,2,4,32,2048]{4,3,2,1,0:T(8,128)(2,1)S(1)} %get-tuple-element.16) | copy-start | bytes 12582916
where the time goes:
time: 134 us; the launch traced here: 133 us
  Pallas kernels  115 us (86%)
  local copies, waits for them, and re-layouts  8.39 us (6%)
  matrix products  7.5 us (6%)
  other arithmetic  1.81 us (1%)
    pallas_call x2, Pallas kernels, call(): pl.pallas_call(kernel, out_shape=outs, in_specs=[VM] * len(args), out_spe...  115 us
    unnamed x37, local copies, waits for them, and re-layouts  6.36 us
    dot_general x1, matrix products, shards(): jnp.dot(token_rows, ow_all.reshape(-1, width), preferred_element_type=f32)  3.73 us

commit v1 on v0

v1 whole, which is shorter than its diff:
```python
import math

import jax
import jax.numpy as jnp
import numpy as np
from jax import lax
from jax.experimental import pallas as pl
from jax.experimental.pallas import tpu as pltpu
from jax.sharding import PartitionSpec as P

NOPE = 64
ROPE = 32
VDIM = 64
GRID_W = 64
TOK_DEV = 1024
CTX_DEV = 32
CORES = 2
KD = NOPE + ROPE
WIDE = KD + VDIM

epsilon = 1e-06
theta = 10000.0

NT = (((1,), (1,)), ((), ()))
TN = (((0,), (0,)), ((), ()))
TT = (((0,), (1,)), ((), ()))


def axial_tables(count):
    pair_count = ROPE // 4
    positions = np.arange(count)
    frequency = np.power(theta, -np.arange(pair_count, dtype=np.float32) / pair_count).astype(np.float32)
    row_angle = (positions // GRID_W).astype(np.float32)[None, :] * frequency[:, None]
    col_angle = (positions % GRID_W).astype(np.float32)[None, :] * frequency[:, None]
    tables = [np.cos(row_angle), np.sin(row_angle), np.cos(col_angle), np.sin(col_angle)]
    return np.stack(tables).astype(np.float32)


def remote(source, target, send, recv, device):
    return pltpu.make_async_remote_copy(
        src_ref=source,
        dst_ref=target,
        send_sem=send,
        recv_sem=recv,
        device_id=device,
        device_id_type=pl.DeviceIdType.MESH,
    )


def loop(low, high, body):
    def step(k, carry):
        body(k)
        return carry

    lax.fori_loop(low, high, step, 0)


class Here:
    def __init__(self):
        self.sp, self.tp = lax.axis_index("sp"), lax.axis_index("tp")
        self.S, self.T = lax.axis_size("sp"), lax.axis_size("tp")
        self.X = math.isqrt(self.S)
        assert self.X * self.X == self.S
        self.y, self.x = self.sp // self.X, lax.rem(self.sp, self.X)
        self.Z = self.T // CORES
        self.z, self.core = self.tp // CORES, lax.rem(self.tp, CORES)
        self.mate = {"tp": self.tp + 1 - 2 * self.core}

    def greet(self):
        barrier = pltpu.get_barrier_semaphore()
        for k in range(1, self.S):
            to = lax.rem(self.sp + k, self.S)
            pl.semaphore_signal(barrier, inc=1, device_id={"sp": to}, device_id_type=pl.DeviceIdType.MESH)
        for k in range(1, self.T):
            to = lax.rem(self.tp + k, self.T)
            pl.semaphore_signal(barrier, inc=1, device_id={"tp": to}, device_id_type=pl.DeviceIdType.MESH)
        pl.semaphore_wait(barrier, self.S + self.T - 2)

    def block(self, r):
        z, Z = self.z, self.Z
        near = lax.min(z, Z - 1 - z)
        zig = ((r + 1) // 2) * (2 * lax.rem(r, 2) - 1)
        far = (r - near) * jnp.where(z <= Z - 1 - z, 1, -1)
        return z + jnp.where(r <= 2 * near, zig, far)

    def part(self, dy, dx):
        X = self.X
        return lax.rem(self.y + dy + X, X) * X + lax.rem(self.x + dx + X, X)


class Line:
    def __init__(self, at, own, slot, send, recv):
        self.at, self.own, self.slot, self.send, self.recv = at, own, slot, send, recv

    def hop(self, block, step, first=False):
        at = self.at
        to = lax.max(lax.min(at.z + step, at.Z - 1), 0)
        return remote(
            self.own if first else self.slot(block),
            self.slot(block),
            self.send.at[block, (1 - step) // 2],
            self.recv.at[block],
            {"tp": to * CORES + at.core},
        )

    def ends(self, step):
        return (self.at.z + step >= 0) & (self.at.z + step < self.at.Z)

    def start(self):
        for step in (1, -1):

            @pl.when(self.ends(step))
            def _():
                self.hop(self.at.z, step, True).start()

    def way(self, block):
        return jnp.where(block < self.at.z, 1, -1)

    def arrive(self, block):
        step = self.way(block)
        self.hop(block, step).wait_recv()

        @pl.when(self.ends(step))
        def _():
            self.hop(block, step).start()

    def drain(self):
        for step in (1, -1):

            @pl.when(self.ends(step))
            def _():
                self.hop(self.at.z, step, True).wait_send()

        def body(r):
            block = self.at.block(r)
            step = self.way(block)

            @pl.when(self.ends(step))
            def _():
                self.hop(block, step).wait_send()

        loop(1, self.at.Z, body)


class Plane:
    def __init__(self, at, slot, send, recv):
        self.at, self.slot, self.send, self.recv = at, slot, send, recv

    def side(self, b):
        return lax.rem(b + self.at.core, 2)

    def place(self, e, i, j):
        return self.at.part(i * e + j * (1 - e), i * (1 - e) + j * e)

    def copy(self, b, s, to, sem):
        return remote(self.slot(b, s), self.slot(b, s), self.send.at[b, sem], self.recv.at[b, s], {"sp": to})

    def sends(self, b, first, second, act):
        X, e = self.at.X, self.side(b)
        if first:
            for i in range(1, X):
                act(self.copy(b, self.at.sp, self.place(e, i, 0), i - 1))
            for j in range(1, X):
                act(self.copy(b, self.at.sp, self.place(e, 0, j), X + j - 2))
        if second:
            for i in range(1, X):
                for j in range(1, X):
                    sem = 2 * (X - 1) + (i - 1) * (X - 1) + j - 1
                    act(self.copy(b, self.place(e, -i, 0), self.place(e, 0, j), sem))

    def push(self, b):
        self.sends(b, True, False, lambda copy: copy.start())

    def take(self, b, s):
        self.copy(b, s, self.place(0, 1, 0), 0).wait_recv()

    def forward(self, b, then=None):
        e = self.side(b)
        for i in range(1, self.at.X):
            s = self.place(e, -i, 0)
            self.take(b, s)
            if then is not None:
                then(b, s)
        self.sends(b, False, True, lambda copy: copy.start())

    def rest(self, b):
        e = self.side(b)
        for j in range(1, self.at.X):
            for i in range(self.at.X):
                self.take(b, self.place(e, -i, -j))

    def drain(self, b):
        self.sends(b, True, True, lambda copy: copy.wait_send())


class Mate:
    def __init__(self, at, slot, send, recv):
        self.at, self.slot, self.send, self.recv = at, slot, send, recv

    def copy(self, core, *key):
        return remote(self.slot(core, *key), self.slot(core, *key), self.send.at[key], self.recv.at[key], self.at.mate)

    def give(self, *key):
        self.copy(self.at.core, *key).start()

    def take(self, *key):
        self.copy(1 - self.at.core, *key).wait_recv()

    def drain(self, *key):
        self.copy(self.at.core, *key).wait_send()


def rms(tensor, axis):
    return tensor * lax.rsqrt(jnp.mean(tensor * tensor, axis=axis, keepdims=True) + epsilon)


def kernel(
    vectors, gain_q, gain_k, shift,
    latent, context, mod_weight, dq, dkv, ow, rope_w, uq, uk, uv, tables_in,
    out,
    lat, con, mw, rope, up_q, up_k, up_v, tables, uq_t, ukv_t,
    dq_all, dkv_all, ow_all, pm, msum, mods, normed,
    kv_lats, q_lats, ctx_lats, q, kv, ctx_kv, m_scr, l_scr, acc, att, att_in,
    local, p_send, p_recv, t_send, t_recv,
    wl_send, wl_recv, wp_send, wp_recv, wm_send, wm_recv,
    ll_send, ll_recv, lp_send, lp_recv, lm_send, lm_recv, qm_send, qm_recv,
    x_send, x_recv, a_send, a_recv,
):
    at = Here()
    sp, tp, S, T, Z, z, core = at.sp, at.tp, at.S, at.T, at.Z, at.z, at.core
    f32, bf16 = jnp.float32, jnp.bfloat16
    H, N, _ = q.shape
    rows = out.shape[0]
    span = rows * CORES
    ctx_rows = con.shape[0]
    rank = uk.shape[0]
    width = latent.shape[1]
    TQ = span
    factor = KD ** (-0.5) * math.log2(math.e)

    loads = [
        pltpu.make_async_copy(a, b, local.at[i])
        for i, (a, b) in enumerate((
            (mod_weight, mw), (latent, lat), (context, con), (rope_w, rope), (uq, up_q), (uk, up_k), (uv, up_v),
            (tables_in, tables), (dq, dq_all.at[z, core]), (dkv, dkv_all.at[z, core]), (ow, ow_all.at[z, core]),
        ))
    ]
    for copy in loads:
        copy.start()
    at.greet()

    weights = ((dq, dq_all), (dkv, dkv_all), (ow, ow_all))
    w_lines, w_planes, w_mates = [], [], []
    for i, (own, every) in enumerate(weights):
        w_lines.append(Line(
            at, own.at[sp], (lambda e: lambda b: e.at[b, core, sp])(every), wl_send.at[i], wl_recv.at[i]
        ))
        w_planes.append(Plane(at, (lambda e: lambda b, s: e.at[b, core, s])(every), wp_send.at[i], wp_recv.at[i]))
        w_mates.append(Mate(at, (lambda e: lambda c, b: e.at[b, c])(every), wm_send.at[i], wm_recv.at[i]))

    def own_mate(i):
        own, every = weights[i]
        return remote(own, every.at[z, core], wm_send.at[i, z], wm_recv.at[i, z], at.mate)

    for i in range(2):
        w_lines[i].start()

    span_k = mw.shape[1]

    def silu(v):
        return v / (1.0 + jnp.exp(-v))

    where = pl.ds(pl.multiple_of(sp * span_k, span_k), span_k)
    wide = [jnp.broadcast_to(silu(vectors[i : i + 1, where]), (8, span_k)) for i in range(2)]
    index = lax.broadcasted_iota(jnp.int32, (8, span_k), 0)
    loads[0].wait()
    part = jnp.zeros(pm.shape[1:], f32)
    for r in range(mw.shape[0]):
        act = jnp.where(index == 2 * r, wide[0], jnp.where(index == 2 * r + 1, wide[1], 0.0)).astype(bf16)
        part = part + jnp.dot(act, mw[r], preferred_element_type=f32)
    pm[sp] = part

    def part_copy(k):
        return remote(pm.at[sp], pm.at[sp], p_send.at[k], p_recv.at[k], {"sp": lax.rem(sp + k, S)})

    def part_wait(k):
        to = pm.at[lax.rem(sp - k + S, S)]
        remote(to, to, p_send.at[k], p_recv.at[k], {"sp": lax.rem(sp + k, S)}).wait_recv()

    def mod_copy(k):
        return remote(msum, mods.at[tp], t_send.at[k], t_recv.at[k], {"tp": lax.rem(tp + k, T)})

    def mod_wait(k):
        to = mods.at[lax.rem(tp - k + T, T)]
        remote(to, to, t_send.at[k], t_recv.at[k], {"tp": lax.rem(tp + k, T)}).wait_recv()

    loop(1, S, lambda k: part_copy(k).start())
    for i in range(2):
        own_mate(i).start()
    loop(1, S, part_wait)
    total = pm[0]
    for k in range(1, S):
        total = total + pm[k]
    msum[...] = total
    mods[tp] = total
    loop(1, T, lambda k: mod_copy(k).start())

    def weights_arrive(r):
        b = at.block(r)
        for i in range(2):
            w_lines[i].arrive(b)
            w_planes[i].push(b)

    def weights_forward(r):
        b = at.block(r)
        for i in range(2):
            w_planes[i].forward(b)

    for r in range(1, Z):
        weights_arrive(r)
        if r > 1:
            weights_forward(r - 1)
    w_lines[2].start()
    weights_forward(Z - 1)

    for copy in loads[4:7]:
        copy.wait()
    uq_t[...] = up_q[...].astype(f32).T.astype(bf16)
    ukv_t[: H * NOPE, :] = up_k[...].astype(f32).T.astype(bf16)
    ukv_t[H * NOPE :, :] = up_v[...].astype(f32).T.astype(bf16)

    loop(1, T, mod_wait)
    loads[1].wait()
    loads[2].wait()
    gain = vectors[2:3, :]
    every_mod = jnp.concatenate([mods[t] for t in range(T)], axis=1)

    def modulate(source, count, base, kind):
        step = math.gcd(count, 32)
        for i in range(count // step):
            u = source[i * step : (i + 1) * step, :].astype(f32)
            u = rms(u, 1) * gain * (1.0 + every_mod[2 + kind : 3 + kind, :]) + every_mod[kind : kind + 1, :]
            normed[base + i * step : base + (i + 1) * step, :] = u.astype(bf16)

    modulate(lat, rows, 0, 0)
    modulate(con, ctx_rows, rows, 1)

    for r in range(1, Z):
        b = at.block(r)
        w_lines[2].arrive(b)
        for i in range(2):
            w_planes[i].rest(b)
            w_mates[i].give(b)
    for copy in loads[3:4] + loads[7:11]:
        copy.wait()
    for i in range(2):
        for b in range(Z):
            w_mates[i].take(b)

    def tail(u, count):
        u = jnp.concatenate([u, jnp.zeros((count, 128 - ROPE), f32)], axis=1)
        u = jnp.concatenate([u, jnp.zeros((128 - count, 128), f32)], axis=0) if count < 128 else u
        return u.T[:ROPE, :].astype(bf16)

    def put_tail(ref, t):
        ref[-16:, 0:128] = t[:16, :]
        ref[-16:, 128:256] = t[16:, :]

    def get_tail(block, count):
        return jnp.concatenate([block[-16:, 0:128], block[-16:, 128:256]], axis=0)[:, :count]

    stacked = normed[...]
    kv_down = jnp.dot(stacked, dkv_all[...].reshape(width, -1), preferred_element_type=f32)
    kv_latent = (rms(kv_down, 1) * vectors[4:5, :rank]).astype(bf16)
    rope_rows = jnp.dot(stacked, rope[...], preferred_element_type=f32)
    own_kv = kv_lats.at[sp, z, core]
    own_kv[:rows, :] = kv_latent[:rows]
    put_tail(own_kv, tail(rope_rows[:rows], rows))
    own_ctx = ctx_lats.at[sp]
    own_ctx[:ctx_rows, :] = kv_latent[rows:]
    put_tail(own_ctx, tail(rope_rows[rows:], ctx_rows))

    kv_line = Line(at, own_kv, lambda b: kv_lats.at[sp, b, core], ll_send.at[0], ll_recv.at[0])
    kv_plane = Plane(at, lambda b, s: kv_lats.at[s, b, core], lp_send, lp_recv)
    kv_mate = Mate(at, lambda c, s, b: kv_lats.at[s, b, c], lm_send, lm_recv)
    q_line = Line(at, q_lats.at[z, core], lambda b: q_lats.at[b, core], ll_send.at[1], ll_recv.at[1])
    q_mate = Mate(at, lambda c, b: q_lats.at[b, c], qm_send, qm_recv)

    kv_line.start()
    kv_plane.push(z)
    kv_mate.give(sp, z)

    def ctx_copy(k):
        return remote(own_ctx, own_ctx, x_send.at[k], x_recv.at[k], {"sp": lax.rem(sp + k, S)})

    def ctx_wait(k):
        to = ctx_lats.at[lax.rem(sp - k + S, S)]
        remote(to, to, x_send.at[k], x_recv.at[k], {"sp": lax.rem(sp + k, S)}).wait_recv()

    loop(1, S, lambda k: ctx_copy(k).start())

    query_down = jnp.dot(normed[:rows, :], dq_all[...].reshape(width, -1), preferred_element_type=f32)
    q_lats[z, core] = (rms(query_down, 1) * vectors[3:4, : query_down.shape[1]]).astype(bf16)
    q_line.start()
    q_mate.give(z)

    def turned(u, gain, where):
        u = rms(u, 0) * gain[:, :1]
        if where is None:
            return u
        m = ROPE // 4
        a, b, c, d = (u[NOPE + i * m : NOPE + (i + 1) * m, :] for i in range(4))
        rc, rs, cc, cs = (tables[i, :, where] for i in range(4))
        return jnp.concatenate(
            [u[:NOPE, :], a * rc - b * rs, b * rc + a * rs, c * cc - d * cs, d * cc + c * cs], axis=0
        )

    def expand(rows_in, tail_in, to, columns, where):
        u = lax.dot_general(ukv_t[...], rows_in, NT, preferred_element_type=f32)
        for h in range(H):
            key = turned(
                jnp.concatenate([u[h * NOPE : (h + 1) * NOPE, :], tail_in.astype(f32)], axis=0), gain_k[...], where
            )
            to[h * WIDE : h * WIDE + KD, columns] = key.astype(bf16)
            base = H * NOPE + h * VDIM
            to[h * WIDE + KD : (h + 1) * WIDE, columns] = u[base : base + VDIM, :].astype(bf16)

    def kv_forward(r):
        kv_plane.forward(at.block(r), lambda b, s: kv_mate.give(s, b))

    for r in range(1, Z):
        b = at.block(r)
        kv_line.arrive(b)
        kv_plane.push(b)
        kv_mate.give(sp, b)
        kv_forward(r - 1)
    kv_forward(Z - 1)
    for r in range(1, Z):
        w_planes[2].push(at.block(r))
    own_mate(2).start()

    loop(1, S, ctx_wait)
    ctx_block = [ctx_lats[s] for s in range(S)]
    expand(
        jnp.concatenate([block[:ctx_rows, :] for block in ctx_block], axis=0),
        jnp.concatenate([get_tail(block, ctx_rows) for block in ctx_block], axis=1),
        ctx_kv, slice(None), None,
    )

    def chunk(c):
        return at.part(-(c // at.X), -lax.rem(c, at.X))

    def chunk_arrive(c):
        s = chunk(c)

        def body(b):
            e = kv_plane.side(b)
            late = jnp.where(e == 0, c // at.X, lax.rem(c, at.X))

            @pl.when(late != 0)
            def _():
                kv_plane.take(b, s)
                kv_mate.give(s, b)

        loop(0, Z, body)

    def chunk_expand(c):
        s = chunk(c)

        def body(b):
            kv_mate.take(s, b)
            blocks = [kv_lats[s, b, i] for i in range(CORES)]
            expand(
                jnp.concatenate([block[:rows, :] for block in blocks], axis=0),
                jnp.concatenate([get_tail(block, rows) for block in blocks], axis=1),
                kv.at[s],
                pl.ds(pl.multiple_of(b * span, span), span),
                pl.ds(pl.multiple_of(s * N + b * span, span), span),
            )

        loop(0, Z, body)

    def tile_arrive(t):
        b = at.block(t)
        q_line.arrive(b)
        q_mate.give(b)

    def tile_at(t):
        return pl.ds(pl.multiple_of(at.block(t) * TQ, TQ), TQ)

    def lanes(p):
        total = p[:, :128]
        for j in range(1, p.shape[1] // 128):
            total = total + p[:, j * 128 : (j + 1) * 128]
        return total

    def tile_expand(t):
        b = at.block(t)
        q_mate.take(b)
        where = tile_at(t)
        rows_in = q_lats[b].reshape(span, q_lats.shape[3])
        u = lax.dot_general(uq_t[...], rows_in, NT, preferred_element_type=f32)
        for h in range(H):
            spot = pl.ds(pl.multiple_of(sp * N + b * span, span), span)
            query = turned(u[h * KD : (h + 1) * KD, :], gain_q[...], spot)
            query = jnp.concatenate([query, jnp.zeros((128 - KD, span), f32)], axis=0)
            q[h, where, :] = query.T.astype(bf16)
            kt = ctx_kv[h * WIDE : h * WIDE + KD, :]
            vt = ctx_kv[h * WIDE + KD : (h + 1) * WIDE, :]
            s = jnp.dot(q[h, where, :][:, :KD], kt, preferred_element_type=f32) * factor + shift[h : h + 1, :1]
            new = jnp.max(s, axis=1, keepdims=True)
            p = jnp.exp2(s - new)
            m_scr[h, where, :] = jnp.broadcast_to(new, (TQ, 128))
            l_scr[h, where, :] = lanes(p)
            acc[h, where, :] = lax.dot_general(p.astype(bf16), vt, NT, preferred_element_type=f32)

    def pair(t, c):
        where = tile_at(t)
        s_from = chunk(c)
        for h in range(H):
            kt = kv[s_from, h * WIDE : h * WIDE + KD, :]
            vt = kv[s_from, h * WIDE + KD : (h + 1) * WIDE, :]
            s = jnp.dot(q[h, where, :][:, :KD], kt, preferred_element_type=f32) * factor
            old = m_scr[h, where, :][:, :1]
            new = jnp.maximum(old, jnp.max(s, axis=1, keepdims=True))
            scale = jnp.exp2(old - new)
            p = jnp.exp2(s - new)
            m_scr[h, where, :] = jnp.broadcast_to(new, (TQ, 128))
            l_scr[h, where, :] = l_scr[h, where, :] * scale + lanes(p)
            acc[h, where, :] = acc[h, where, :] * scale + lax.dot_general(
                p.astype(bf16), vt, NT, preferred_element_type=f32
            )

    def owner_rows(dest):
        return att.at[pl.ds(pl.multiple_of(dest * rows, rows), rows)]

    def give(dest):
        return remote(owner_rows(dest), att_in.at[tp], a_send.at[dest], a_recv.at[tp], {"tp": dest})

    def finish(t):
        where = tile_at(t)
        heads = [acc[h, where, :] / jnp.sum(l_scr[h, where, :], axis=1, keepdims=True) for h in range(H)]
        att[where, :] = jnp.concatenate(heads, axis=1).astype(bf16)
        for i in range(CORES):
            dest = at.block(t) * CORES + i

            @pl.when(dest != tp)
            def _():
                give(dest).start()

            @pl.when(dest == tp)
            def _():
                att_in[tp] = owner_rows(tp)[...]


    def diagonal(w):
        @pl.when(w < S)
        def _():
            chunk_expand(w)

        @pl.when(w < Z)
        def _():
            tile_expand(w)

        low, high = lax.max(w - S + 1, 0), lax.min(w, Z - 1) + 1

        def one(t):
            pair(t, w - t)

            @pl.when(w - t == S - 1)
            def _():
                finish(t)

        loop(low, high, one)

        @pl.when(w + 1 < S)
        def _():
            chunk_arrive(w + 1)

        @pl.when(w + 1 < Z)
        def _():
            tile_arrive(w + 1)

        @pl.when(w == S - 1)
        def _():
            loop(1, Z, lambda r: w_planes[2].forward(at.block(r)))

    loop(0, Z + S - 1, diagonal)

    def ow_rest(r):
        b = at.block(r)
        w_planes[2].rest(b)
        w_mates[2].give(b)

    loop(1, Z, ow_rest)
    loop(0, Z, lambda b: w_mates[2].take(b))

    def att_wait(k):
        source = lax.rem(tp - k + T, T)
        to = att_in.at[source]
        remote(to, to, a_send.at[source], a_recv.at[source], {"tp": source}).wait_recv()

    loop(1, T, att_wait)
    attended = jnp.concatenate([att_in[t] for t in range(T)], axis=1)
    cut = mods.shape[2]
    for t in range(T):
        where = slice(t * cut, (t + 1) * cut)
        weight = ow_all[:, :, :, :, where].reshape(-1, cut)
        projected = jnp.dot(attended, weight, preferred_element_type=f32)
        out[:, where] = (lat[:, where].astype(f32) + mods[t, 4:5, :] * projected).astype(bf16)

    loop(1, S, lambda k: part_copy(k).wait_send())
    loop(1, T, lambda k: mod_copy(k).wait_send())
    loop(1, S, lambda k: ctx_copy(k).wait_send())
    loop(1, T, lambda k: give(lax.rem(tp + k, T)).wait_send())
    for i in range(3):
        own_mate(i).wait_send()
        w_lines[i].drain()

        def body(r):
            w_planes[i].drain(at.block(r))
            w_mates[i].drain(at.block(r))

        loop(1, Z, body)
    kv_line.drain()
    q_line.drain()

    def body(b):
        kv_plane.drain(b)
        q_mate.drain(b)
        loop(0, S, lambda s: kv_mate.drain(s, b))

    loop(0, Z, body)


DMA = pltpu.SemaphoreType.DMA
VM = pl.BlockSpec(memory_space=pltpu.VMEM)
ANY = pl.BlockSpec(memory_space=pl.ANY)


def shards(
    latent, context, cond, cond_context, mod_weight, norm_gain, down_q, down_kv, rope_weight, qlat_gain, kvlat_gain,
    up_query, up_key, up_value, query_gain, key_gain, context_bias, out_weight,
):
    S, T = lax.axis_size("sp"), lax.axis_size("tp")
    Z = T // CORES
    bf16, f32 = jnp.bfloat16, jnp.float32
    own_rows, width = latent.shape
    ctx_rows = context.shape[0]
    N = own_rows * T
    cols = mod_weight.shape[2]
    dq, dkv, ow = (w.reshape(S, w.shape[0] // S, w.shape[1]) for w in (down_q, down_kv, out_weight))
    QR, KR = down_q.shape[1], down_kv.shape[1]
    H = up_key.shape[1] // NOPE

    def row(v):
        return jnp.pad(v.astype(f32), (0, width - v.shape[0]))[None, :]

    vectors = jnp.concatenate(
        [row(v) for v in (cond, cond_context, norm_gain, qlat_gain, kvlat_gain)] + [jnp.zeros((3, width), f32)], axis=0
    )
    gain_q = jnp.broadcast_to(query_gain[:, None], (KD, 128))
    gain_k = jnp.broadcast_to(key_gain[:, None], (KD, 128))
    shift = (context_bias + math.log(TOK_DEV / CTX_DEV)) * math.log2(math.e)
    shift = jnp.broadcast_to(shift[:, None], (H, 128))
    tables = jnp.asarray(axial_tables(S * N))
    args = (
        vectors, gain_q, gain_k, shift, latent, context, mod_weight, dq, dkv, ow, rope_weight,
        up_query, up_key, up_value, tables,
    )
    lat_rows, kv_rows = own_rows + 16, H * WIDE
    V = pltpu.VMEM
    scratch = [
        V(latent.shape, bf16), V(context.shape, bf16), V(mod_weight.shape, bf16), V(rope_weight.shape, bf16),
        V(up_query.shape, bf16), V(up_key.shape, bf16), V(up_value.shape, bf16), V(tables.shape, f32),
        V(up_query.shape[::-1], bf16), V((H * (NOPE + VDIM), KR), bf16),
        V((Z, CORES) + dq.shape, bf16), V((Z, CORES) + dkv.shape, bf16), V((Z, CORES) + ow.shape, bf16),
        V((S, 8, cols), f32), V((8, cols), f32), V((T, 8, cols), f32), V((own_rows + ctx_rows, width), bf16),
        V((S, Z, CORES, lat_rows, KR), bf16), V((Z, CORES, own_rows, QR), bf16), V((S, ctx_rows + 16, KR), bf16),
        V((H, N, 128), bf16), V((S, kv_rows, N), bf16), V((kv_rows, S * ctx_rows), bf16),
        V((H, N, 128), f32), V((H, N, 128), f32), V((H, N, VDIM), f32),
        V((N, H * VDIM), bf16), V((T, own_rows, H * VDIM), bf16),
        DMA((11,)), DMA((S,)), DMA((S,)), DMA((T,)), DMA((T,)),
        DMA((3, Z, 2)), DMA((3, Z)), DMA((3, Z, S - 1)), DMA((3, Z, S)), DMA((3, Z)), DMA((3, Z)),
        DMA((2, Z, 2)), DMA((2, Z)), DMA((Z, S - 1)), DMA((Z, S)), DMA((S, Z)), DMA((S, Z)), DMA((Z,)), DMA((Z,)),
        DMA((S,)), DMA((S,)), DMA((T,)), DMA((T,)),
    ]
    return pl.pallas_call(
        kernel,
        out_shape=jax.ShapeDtypeStruct(latent.shape, bf16),
        in_specs=[VM] * 4 + [ANY] * 11,
        out_specs=VM,
        scratch_shapes=scratch,
        compiler_params=pltpu.CompilerParams(
            collective_id=1, has_side_effects=True, vmem_limit_bytes=60 * 1024 * 1024
        ),
    )(*args)


def solution(mesh):
    in_specs = (
        P(("sp", "tp"), None),
        P("sp", None),
        P(),
        P(),
        P(None, "sp", "tp"),
        P(),
        P("tp", None),
        P("tp", None),
        P(),
        P(),
        P(),
        P(None, "tp"),
        P(None, "tp"),
        P(None, "tp"),
        P(),
        P(),
        P("tp"),
        P("tp", None),
    )
    out_specs = P(("sp", "tp"), None)
    return jax.shard_map(shards, mesh=mesh, in_specs=in_specs, out_specs=out_specs, check_vma=False)
```

time: 134 us -> 115 us (0.86)
  Pallas kernels: 115 us -> 103 us
  matrix products: 7.5 us -> 0 us
  other arithmetic: 1.81 us -> 4.13 us
    pallas_call x2 -> x1, Pallas kernels: 115 us -> 103 us  [shards(): pl.pallas_call(kernel, out_shape=jax.ShapeDtypeStruct(latent.shape, bf16)...]
    dot_general x6 -> x0, matrix products: 7.5 us -> none  [the longest x1 3.73 us: shards(): jnp.dot(token_rows, ow_all.reshape(-1, width), preferred_element_type=f32)]
    broadcast_in_dim x0 -> x5, other arithmetic: none -> 3.43 us  [row(): return jnp.pad(v.astype(f32), (0, width - v.shape[0]))[None, :]]
    unnamed x37 -> x9, local copies, waits for them, and re-layouts: 6.36 us -> 3.81 us
    another operation x2 -> x0, local copies, waits for them, and re-layouts: 1.43 us -> none  [shards(): jnp.stack([cond, cond_context]).astype(f32)]
where the time goes in v1:
time: 115 us
  Pallas kernels  103 us (90%)
  local copies, waits for them, and re-layouts  7.23 us (6%)
  other arithmetic  4.13 us (4%)
    pallas_call x1, Pallas kernels, shards(): pl.pallas_call(kernel, out_shape=jax.ShapeDtypeStruct(latent.shape, bf16)...  103 us
    unnamed x9, local copies, waits for them, and re-layouts  3.81 us
    broadcast_in_dim x5, other arithmetic, row(): return jnp.pad(v.astype(f32), (0, width - v.shape[0]))[None, :]  3.43 us

profile of v1, /device:TPU:0, one launch (start us, length us, event | category | flops | bytes accessed | tf_op | source)
XLA Modules:
  0.0 114.9 jit_solution(4330863940742865712)
XLA Ops:
  0.0 0.0 copy-start
  0.0 0.7 add_multiply_fusion
  0.7 0.6 broadcast_in_dim.64.shift
  1.4 0.7 broadcast_in_dim.65
  2.0 0.7 broadcast_in_dim.66
  2.7 0.7 broadcast_in_dim.67
  3.4 0.7 pad_convert_fusion.1
  4.1 0.7 pad_convert_fusion
  4.8 0.7 concatenate.3.vectors
  5.5 0.0 copy-start.2
  5.5 1.4 %broadcast_in_dim.62.gain_q = f32[96,128]{1,0:T(8,128)} broadcast(f32[96]{0:T(128)} %param.33), dimensions={0} | broadcast | bytes 49536 | tf_op jit(solution)/shard_map/broadcast_in_dim | solution.py:662
  6.9 0.0 copy-done.2
  6.9 0.7 broadcast_in_dim.63.gain_k
  7.6 0.0 copy-done
  7.6 0.0 copy-start.1
  7.6 0.9 copy.21.uq
  8.5 0.0 copy-done.1
  8.5 1.0 copy.20.rope_w
  9.5 103.5 %shard_map.181 = bf16[128,2048]{1,0:T(8,128)(2,1)} custom-call(f32[8,2048]{1,0:T(8,128)} %concatenate.3.vectors, f32[96,128]{1,0:T(8,128)} %broadcast_in_dim.62.gain_q, f32[96,128]{1,0:T(8,128)} %broadcast_in_dim.63.gain_k, f32[2,128]{1,0:T(2,128)} %broadcast_in_dim.64.shift, bf16[128,2048]{1,0:T(8,128)(2,1)} %latent.1, bf16[32,2048]{1,0:T(8,128)(2,1)} %context.1, ...), custom_call_target="tpu_custom_call" | custom-call | tf_op jit(solution)/shard_map/pallas_call | solution.py:688
  113.0 1.9 %copy.23 = bf16[128,2048]{1,0:T(8,128)(2,1)} copy(bf16[128,2048]{1,0:T(8,128)(2,1)} %shard_map.181) | data formatting | bytes 1048576
  (1 shorter events, 0.0 us)
Async XLA Ops:
  0.0 7.6 %copy-start = (bf16[768,192]{0,1:T(8,128)(2,1)S(1)}, bf16[768,192]{0,1:T(8,128)(2,1)}, u32[]{:S(2)}) copy-start(bf16[768,192]{0,1:T(8,128)(2,1)} %param.30) | copy-start | bytes 884740
  5.5 1.4 %copy-start.2 = (f32[96]{0:T(128)S(1)}, f32[96]{0:T(128)}, u32[]{:S(2)}) copy-start(f32[96]{0:T(128)} %param.34) | copy-start | bytes 1156
  7.6 0.9 copy-start.1

commit v2 on v1

--- a/solution.py
+++ b/solution.py
@@ -140,6 +140,21 @@
                 self.hop(block, step).wait_send()
 
         loop(1, self.at.Z, body)
+
+
+class Direct(Line):
+    def hop(self, block, to):
+        at = self.at
+        return remote(self.own, self.slot(block), self.send.at[to, 0], self.recv.at[block], {"tp": to * CORES + at.core})
+
+    def start(self):
+        loop(1, self.at.Z, lambda r: self.hop(self.at.z, self.at.block(r)).start())
+
+    def arrive(self, block):
+        self.hop(block, self.at.z).wait_recv()
+
+    def drain(self):
+        loop(1, self.at.Z, lambda r: self.hop(self.at.z, self.at.block(r)).wait_send())
 
 
 class Plane:
@@ -215,12 +230,13 @@
 
 
 def kernel(
-    vectors, gain_q, gain_k, shift,
-    latent, context, mod_weight, dq, dkv, ow, rope_w, uq, uk, uv, tables_in,
+    cond_in, cond_context_in, gain_in, qlat_in, kvlat_in, gain_q_in, gain_k_in, bias_in,
+    latent, context, mod_weight, dq, dkv, ow, rope_t, uq_t_in, uk, uv, tables_in,
     out,
-    lat, con, mw, rope, up_q, up_k, up_v, tables, uq_t, ukv_t,
+    cond, cond_context, norm_gain, qlat_gain, kvlat_gain, gain_row, bias,
+    lat, con, mw, rope, uq_t, up_k, up_v, tables, uk_t, gains,
     dq_all, dkv_all, ow_all, pm, msum, mods, normed,
-    kv_lats, q_lats, ctx_lats, q, kv, ctx_kv, m_scr, l_scr, acc, att, att_in,
+    kv_lats, q_lats, ctx_lats, q, keys, values, ctx_kv, ctx_values, m_scr, acc, att, att_in,
     local, p_send, p_recv, t_send, t_recv,
     wl_send, wl_recv, wp_send, wp_recv, wm_send, wm_recv,
     ll_send, ll_recv, lp_send, lp_recv, lm_send, lm_recv, qm_send, qm_recv,
@@ -233,26 +249,31 @@
     rows = out.shape[0]
     span = rows * CORES
     ctx_rows = con.shape[0]
-    rank = uk.shape[0]
     width = latent.shape[1]
-    TQ = span
+    G = 2 if Z % 2 == 0 else 1
+    TQ = span * G
+    LAG = 2
+    tiles = Z // G
     factor = KD ** (-0.5) * math.log2(math.e)
 
     loads = [
         pltpu.make_async_copy(a, b, local.at[i])
         for i, (a, b) in enumerate((
-            (mod_weight, mw), (latent, lat), (context, con), (rope_w, rope), (uq, up_q), (uk, up_k), (uv, up_v),
-            (tables_in, tables), (dq, dq_all.at[z, core]), (dkv, dkv_all.at[z, core]), (ow, ow_all.at[z, core]),
+            (mod_weight, mw), (cond_in, cond), (cond_context_in, cond_context),
+            (latent, lat), (context, con), (gain_in, norm_gain),
+            (uq_t_in, uq_t), (uk, up_k), (uv, up_v), (rope_t, rope), (qlat_in, qlat_gain), (kvlat_in, kvlat_gain),
+            (gain_q_in, gain_row.at[0]), (gain_k_in, gain_row.at[1]), (bias_in, bias), (tables_in, tables),
+            (dq, dq_all.at[z, core]), (dkv, dkv_all.at[z, core]), (ow, ow_all.at[z, core]),
         ))
     ]
     for copy in loads:
         copy.start()
     at.greet()
 
-    weights = ((dq, dq_all), (dkv, dkv_all), (ow, ow_all))
+    weights = ((dkv, dkv_all), (dq, dq_all), (ow, ow_all))
     w_lines, w_planes, w_mates = [], [], []
     for i, (own, every) in enumerate(weights):
-        w_lines.append(Line(
+        w_lines.append((Direct if i == 0 else Line)(
             at, own.at[sp], (lambda e: lambda b: e.at[b, core, sp])(every), wl_send.at[i], wl_recv.at[i]
         ))
         w_planes.append(Plane(at, (lambda e: lambda b, s: e.at[b, core, s])(every), wp_send.at[i], wp_recv.at[i]))
@@ -270,10 +291,20 @@
     def silu(v):
         return v / (1.0 + jnp.exp(-v))
 
-    where = pl.ds(pl.multiple_of(sp * span_k, span_k), span_k)
-    wide = [jnp.broadcast_to(silu(vectors[i : i + 1, where]), (8, span_k)) for i in range(2)]
+    def row(ref):
+        block = ref[...].astype(f32)
+        return jnp.concatenate([block[i : i + 1, :] for i in range(block.shape[0])], axis=1)
+
+    for copy in loads[:3]:
+        copy.wait()
+    wide = []
+    for ref in (cond, cond_context):
+        every = row(ref)
+        mine = every[:, :span_k]
+        for i in range(1, S):
+            mine = jnp.where(sp == i, every[:, i * span_k : (i + 1) * span_k], mine)
+        wide.append(jnp.broadcast_to(silu(mine), (8, span_k)))
     index = lax.broadcasted_iota(jnp.int32, (8, span_k), 0)
-    loads[0].wait()
     part = jnp.zeros(pm.shape[1:], f32)
     for r in range(mw.shape[0]):
         act = jnp.where(index == 2 * r, wide[0], jnp.where(index == 2 * r + 1, wide[1], 0.0)).astype(bf16)
@@ -323,16 +354,16 @@
     w_lines[2].start()
     weights_forward(Z - 1)
 
-    for copy in loads[4:7]:
+    for copy in loads[3:16]:
         copy.wait()
-    uq_t[...] = up_q[...].astype(f32).T.astype(bf16)
-    ukv_t[: H * NOPE, :] = up_k[...].astype(f32).T.astype(bf16)
-    ukv_t[H * NOPE :, :] = up_v[...].astype(f32).T.astype(bf16)
+    uk_t[...] = up_k[...].astype(f32).T.astype(bf16)
+    for i in range(2):
+        line = jnp.concatenate([gain_row[i], jnp.zeros((1, 128 - KD), f32)], axis=1)
+        gains[i] = jnp.broadcast_to(line, (128, 128)).T[:KD, :]
+    shift = [(bias[:, h : h + 1] + math.log(TOK_DEV / CTX_DEV)) * math.log2(math.e) for h in range(H)]
 
     loop(1, T, mod_wait)
-    loads[1].wait()
-    loads[2].wait()
-    gain = vectors[2:3, :]
+    gain = row(norm_gain)
     every_mod = jnp.concatenate([mods[t] for t in range(T)], axis=1)
 
     def modulate(source, count, base, kind):
@@ -345,40 +376,36 @@
     modulate(lat, rows, 0, 0)
     modulate(con, ctx_rows, rows, 1)
 
-    for r in range(1, Z):
-        b = at.block(r)
-        w_lines[2].arrive(b)
-        for i in range(2):
+    def gather_rest(i):
+        for r in range(1, Z):
+            b = at.block(r)
             w_planes[i].rest(b)
             w_mates[i].give(b)
-    for copy in loads[3:4] + loads[7:11]:
-        copy.wait()
-    for i in range(2):
         for b in range(Z):
             w_mates[i].take(b)
 
-    def tail(u, count):
-        u = jnp.concatenate([u, jnp.zeros((count, 128 - ROPE), f32)], axis=1)
-        u = jnp.concatenate([u, jnp.zeros((128 - count, 128), f32)], axis=0) if count < 128 else u
-        return u.T[:ROPE, :].astype(bf16)
+    gather_rest(0)
+    for copy in loads[16:]:
+        copy.wait()
 
     def put_tail(ref, t):
-        ref[-16:, 0:128] = t[:16, :]
-        ref[-16:, 128:256] = t[16:, :]
+        base, count = ref.shape[0] - 16, t.shape[1]
+        ref[base:, 0:count] = t[:16, :]
+        ref[base:, 128 : 128 + count] = t[16:, :]
 
     def get_tail(block, count):
         return jnp.concatenate([block[-16:, 0:128], block[-16:, 128:256]], axis=0)[:, :count]
 
     stacked = normed[...]
     kv_down = jnp.dot(stacked, dkv_all[...].reshape(width, -1), preferred_element_type=f32)
-    kv_latent = (rms(kv_down, 1) * vectors[4:5, :rank]).astype(bf16)
-    rope_rows = jnp.dot(stacked, rope[...], preferred_element_type=f32)
+    kv_latent = (rms(kv_down, 1) * row(kvlat_gain)).astype(bf16)
+    rope_rows = lax.dot_general(rope[...], stacked, NT, preferred_element_type=f32).astype(bf16)
     own_kv = kv_lats.at[sp, z, core]
     own_kv[:rows, :] = kv_latent[:rows]
-    put_tail(own_kv, tail(rope_rows[:rows], rows))
+    put_tail(own_kv, rope_rows[:, :rows])
     own_ctx = ctx_lats.at[sp]
     own_ctx[:ctx_rows, :] = kv_latent[rows:]
-    put_tail(own_ctx, tail(rope_rows[rows:], ctx_rows))
+    put_tail(own_ctx, rope_rows[:, rows:])
 
     kv_line = Line(at, own_kv, lambda b: kv_lats.at[sp, b, core], ll_send.at[0], ll_recv.at[0])
     kv_plane = Plane(at, lambda b, s: kv_lats.at[s, b, core], lp_send, lp_recv)
@@ -399,8 +426,9 @@
 
     loop(1, S, lambda k: ctx_copy(k).start())
 
+    gather_rest(1)
     query_down = jnp.dot(normed[:rows, :], dq_all[...].reshape(width, -1), preferred_element_type=f32)
-    q_lats[z, core] = (rms(query_down, 1) * vectors[3:4, : query_down.shape[1]]).astype(bf16)
+    q_lats[z, core] = (rms(query_down, 1) * row(qlat_gain)).astype(bf16)
     q_line.start()
     q_mate.give(z)
 
@@ -415,177 +443,207 @@
             [u[:NOPE, :], a * rc - b * rs, b * rc + a * rs, c * cc - d * cs, d * cc + c * cs], axis=0
         )
 
-    def expand(rows_in, tail_in, to, columns, where):
-        u = lax.dot_general(ukv_t[...], rows_in, NT, preferred_element_type=f32)
+    def expand_keys(rows_in, tail_in, put, where):
+        u = lax.dot_general(uk_t[...], rows_in, NT, preferred_element_type=f32)
         for h in range(H):
-            key = turned(
-                jnp.concatenate([u[h * NOPE : (h + 1) * NOPE, :], tail_in.astype(f32)], axis=0), gain_k[...], where
-            )
-            to[h * WIDE : h * WIDE + KD, columns] = key.astype(bf16)
-            base = H * NOPE + h * VDIM
-            to[h * WIDE + KD : (h + 1) * WIDE, columns] = u[base : base + VDIM, :].astype(bf16)
-
-    def kv_forward(r):
-        kv_plane.forward(at.block(r), lambda b, s: kv_mate.give(s, b))
-
-    for r in range(1, Z):
+            key = jnp.concatenate([u[h * NOPE : (h + 1) * NOPE, :], tail_in.astype(f32)], axis=0)
+            put(h, turned(key, gains[1], where).astype(bf16))
+
+    def expand_values(rows_in, put):
+        u = jnp.dot(rows_in, up_v[...], preferred_element_type=f32).astype(bf16)
+        ones = jnp.ones((rows_in.shape[0], 128 - VDIM), bf16)
+        for h in range(H):
+            put(h, jnp.concatenate([u[:, h * VDIM : (h + 1) * VDIM], ones], axis=1))
+
+    def joined(blocks, count):
+        return (
+            jnp.concatenate([block[:count, :] for block in blocks], axis=0),
+            jnp.concatenate([get_tail(block, count) for block in blocks], axis=1),
+        )
+
+    def kv_arrive(r):
         b = at.block(r)
         kv_line.arrive(b)
         kv_plane.push(b)
         kv_mate.give(sp, b)
-        kv_forward(r - 1)
-    kv_forward(Z - 1)
-    for r in range(1, Z):
-        w_planes[2].push(at.block(r))
-    own_mate(2).start()
-
-    loop(1, S, ctx_wait)
-    ctx_block = [ctx_lats[s] for s in range(S)]
-    expand(
-        jnp.concatenate([block[:ctx_rows, :] for block in ctx_block], axis=0),
-        jnp.concatenate([get_tail(block, ctx_rows) for block in ctx_block], axis=1),
-        ctx_kv, slice(None), None,
-    )
-
-    def chunk(c):
-        return at.part(-(c // at.X), -lax.rem(c, at.X))
-
-    def chunk_arrive(c):
-        s = chunk(c)
-
-        def body(b):
-            e = kv_plane.side(b)
-            late = jnp.where(e == 0, c // at.X, lax.rem(c, at.X))
-
-            @pl.when(late != 0)
-            def _():
+
+    def kv_forward(r):
+        kv_plane.forward(at.block(r), lambda b, s: kv_mate.give(s, b))
+
+    def kv_rest(r):
+        b = at.block(r)
+        e = kv_plane.side(b)
+        for j in range(1, at.X):
+            for i in range(at.X):
+                s = kv_plane.place(e, -i, -j)
                 kv_plane.take(b, s)
                 kv_mate.give(s, b)
 
-        loop(0, Z, body)
-
     def chunk_expand(c):
-        s = chunk(c)
-
-        def body(b):
+        b = at.block(c)
+
+        def body(s):
             kv_mate.take(s, b)
-            blocks = [kv_lats[s, b, i] for i in range(CORES)]
-            expand(
-                jnp.concatenate([block[:rows, :] for block in blocks], axis=0),
-                jnp.concatenate([get_tail(block, rows) for block in blocks], axis=1),
-                kv.at[s],
-                pl.ds(pl.multiple_of(b * span, span), span),
-                pl.ds(pl.multiple_of(s * N + b * span, span), span),
-            )
-
-        loop(0, Z, body)
-
-    def tile_arrive(t):
-        b = at.block(t)
+            rows_in, tail_in = joined([kv_lats[s, b, i] for i in range(CORES)], rows)
+            here = pl.ds(pl.multiple_of(s * span, span), span)
+
+            def put_key(h, key):
+                keys[c, h, :, here] = key
+
+            def put_value(h, value):
+                values[c, h, here, :] = value
+
+            expand_keys(rows_in, tail_in, put_key, pl.ds(pl.multiple_of(s * N + b * span, span), span))
+            expand_values(rows_in, put_value)
+
+        loop(0, S, body)
+
+    def q_arrive(r):
+        b = at.block(r)
         q_line.arrive(b)
         q_mate.give(b)
 
     def tile_at(t):
-        return pl.ds(pl.multiple_of(at.block(t) * TQ, TQ), TQ)
-
-    def lanes(p):
-        total = p[:, :128]
-        for j in range(1, p.shape[1] // 128):
-            total = total + p[:, j * 128 : (j + 1) * 128]
-        return total
+        return pl.ds(pl.multiple_of(t * TQ, TQ), TQ)
+
+    def absorb(where, kts, vts, shifts, first):
+        scores = [jnp.dot(q[h, where, :][:, :KD], kts[h], preferred_element_type=f32) for h in range(H)]
+        olds = [None if first else m_scr[h, where, :][:, :1] for h in range(H)]
+        accs = [None if first else acc[h, where, :] for h in range(H)]
+        news, sums = [], []
+        for h in range(H):
+            s = scores[h]
+            new = jnp.max(s, axis=1, keepdims=True) * factor
+            if shifts is not None:
+                new = new + shifts[h]
+            base = new
+            if not first:
+                new = jnp.maximum(olds[h], new)
+            base = new if shifts is None else new - shifts[h]
+            p = jnp.exp2(s * factor - base)
+            o = jnp.dot(p.astype(bf16), vts[h], preferred_element_type=f32)
+            news.append(new)
+            sums.append(o if first else accs[h] * jnp.exp2(olds[h] - new) + o)
+        for h in range(H):
+            m_scr[h, where, :] = jnp.broadcast_to(news[h], (TQ, 128))
+            acc[h, where, :] = sums[h]
 
     def tile_expand(t):
-        b = at.block(t)
-        q_mate.take(b)
-        where = tile_at(t)
-        rows_in = q_lats[b].reshape(span, q_lats.shape[3])
-        u = lax.dot_general(uq_t[...], rows_in, NT, preferred_element_type=f32)
-        for h in range(H):
+        for g in range(G):
+            b = at.block(t * G + g)
+            q_mate.take(b)
+            rows_in = q_lats[b].reshape(span, q_lats.shape[3])
+            u = lax.dot_general(uq_t[...], rows_in, NT, preferred_element_type=f32)
             spot = pl.ds(pl.multiple_of(sp * N + b * span, span), span)
-            query = turned(u[h * KD : (h + 1) * KD, :], gain_q[...], spot)
-            query = jnp.concatenate([query, jnp.zeros((128 - KD, span), f32)], axis=0)
-            q[h, where, :] = query.T.astype(bf16)
-            kt = ctx_kv[h * WIDE : h * WIDE + KD, :]
-            vt = ctx_kv[h * WIDE + KD : (h + 1) * WIDE, :]
-            s = jnp.dot(q[h, where, :][:, :KD], kt, preferred_element_type=f32) * factor + shift[h : h + 1, :1]
-            new = jnp.max(s, axis=1, keepdims=True)
-            p = jnp.exp2(s - new)
-            m_scr[h, where, :] = jnp.broadcast_to(new, (TQ, 128))
-            l_scr[h, where, :] = lanes(p)
-            acc[h, where, :] = lax.dot_general(p.astype(bf16), vt, NT, preferred_element_type=f32)
+            where = pl.ds(pl.multiple_of(t * TQ + g * span, span), span)
+            for h in range(H):
+                query = turned(u[h * KD : (h + 1) * KD, :], gains[0], spot)
+                query = jnp.concatenate([query, jnp.zeros((128 - KD, span), f32)], axis=0)
+                q[h, where, :] = query.T.astype(bf16)
+        absorb(
+            tile_at(t), [ctx_kv[h, :KD, :] for h in range(H)],
+            [ctx_values[h] for h in range(H)], shift, True,
+        )
 
     def pair(t, c):
-        where = tile_at(t)
-        s_from = chunk(c)
-        for h in range(H):
-            kt = kv[s_from, h * WIDE : h * WIDE + KD, :]
-            vt = kv[s_from, h * WIDE + KD : (h + 1) * WIDE, :]
-            s = jnp.dot(q[h, where, :][:, :KD], kt, preferred_element_type=f32) * factor
-            old = m_scr[h, where, :][:, :1]
-            new = jnp.maximum(old, jnp.max(s, axis=1, keepdims=True))
-            scale = jnp.exp2(old - new)
-            p = jnp.exp2(s - new)
-            m_scr[h, where, :] = jnp.broadcast_to(new, (TQ, 128))
-            l_scr[h, where, :] = l_scr[h, where, :] * scale + lanes(p)
-            acc[h, where, :] = acc[h, where, :] * scale + lax.dot_general(
-                p.astype(bf16), vt, NT, preferred_element_type=f32
-            )
-
-    def owner_rows(dest):
-        return att.at[pl.ds(pl.multiple_of(dest * rows, rows), rows)]
-
-    def give(dest):
-        return remote(owner_rows(dest), att_in.at[tp], a_send.at[dest], a_recv.at[tp], {"tp": dest})
+        absorb(tile_at(t), [keys[c, h] for h in range(H)], [values[c, h] for h in range(H)], None, False)
+
+    def owner_rows(r, i):
+        return att.at[pl.ds(pl.multiple_of(r * span + i * rows, rows), rows)]
+
+    def give(r, i):
+        dest = at.block(r) * CORES + i
+        return remote(owner_rows(r, i), att_in.at[tp], a_send.at[dest], a_recv.at[tp], {"tp": dest})
 
     def finish(t):
         where = tile_at(t)
-        heads = [acc[h, where, :] / jnp.sum(l_scr[h, where, :], axis=1, keepdims=True) for h in range(H)]
+        parts = [acc[h, where, :] for h in range(H)]
+        heads = [part[:, :VDIM] / part[:, VDIM : 2 * VDIM] for part in parts]
         att[where, :] = jnp.concatenate(heads, axis=1).astype(bf16)
-        for i in range(CORES):
-            dest = at.block(t) * CORES + i
-
-            @pl.when(dest != tp)
-            def _():
-                give(dest).start()
-
-            @pl.when(dest == tp)
-            def _():
-                att_in[tp] = owner_rows(tp)[...]
-
-
-    def diagonal(w):
-        @pl.when(w < S)
+        for g in range(G):
+            r = t * G + g
+            for i in range(CORES):
+
+                @pl.when((at.block(r) != z) | (core != i))
+                def _():
+                    give(r, i).start()
+
+                @pl.when((at.block(r) == z) & (core == i))
+                def _():
+                    att_in[tp] = owner_rows(r, i)[...]
+
+    for r in range(1, 3):
+        if r < Z:
+            w_lines[2].arrive(at.block(r))
+            kv_arrive(r)
+        if r - 1 < Z:
+            kv_forward(r - 1)
+        if r >= 2:
+            kv_rest(r - 2)
+    own_mate(2).start()
+
+    loop(1, S, ctx_wait)
+    rows_in, tail_in = joined([ctx_lats[s] for s in range(S)], ctx_rows)
+
+    def put_ctx_key(h, key):
+        ctx_kv[h, :KD, :] = key
+
+    def put_ctx_value(h, value):
+        ctx_values[h] = value
+
+    expand_keys(rows_in, tail_in, put_ctx_key, None)
+    expand_values(rows_in, put_ctx_value)
+
+    steps = Z + LAG * (tiles - 1)
+
+    def step(w):
+        k = w + 3
+
+        @pl.when(w + 1 < Z)
+        def _():
+            q_arrive(w + 1)
+
+        @pl.when(k < Z)
+        def _():
+            w_lines[2].arrive(at.block(k))
+            kv_arrive(k)
+
+        @pl.when(k - 1 < Z)
+        def _():
+            kv_forward(k - 1)
+
+        @pl.when(k - 1 == Z - 1)
+        def _():
+            loop(1, Z, lambda r: w_planes[2].push(at.block(r)))
+
+        @pl.when(k - 2 < Z)
+        def _():
+            kv_rest(k - 2)
+
+        @pl.when(k - 2 == Z)
+        def _():
+            loop(1, Z, lambda r: w_planes[2].forward(at.block(r)))
+
+        @pl.when(w < Z)
         def _():
             chunk_expand(w)
 
-        @pl.when(w < Z)
-        def _():
-            tile_expand(w)
-
-        low, high = lax.max(w - S + 1, 0), lax.min(w, Z - 1) + 1
-
-        def one(t):
-            pair(t, w - t)
-
-            @pl.when(w - t == S - 1)
+        for t in range(tiles):
+            c = w - LAG * t
+
+            @pl.when(c == 0)
+            def _():
+                tile_expand(t)
+
+            @pl.when((c >= 0) & (c < Z))
+            def _():
+                pair(t, c)
+
+            @pl.when(c == Z - 1)
             def _():
                 finish(t)
 
-        loop(low, high, one)
-
-        @pl.when(w + 1 < S)
-        def _():
-            chunk_arrive(w + 1)
-
-        @pl.when(w + 1 < Z)
-        def _():
-            tile_arrive(w + 1)
-
-        @pl.when(w == S - 1)
-        def _():
-            loop(1, Z, lambda r: w_planes[2].forward(at.block(r)))
-
-    loop(0, Z + S - 1, diagonal)
+    loop(0, steps, step)
 
     def ow_rest(r):
         b = at.block(r)
@@ -612,7 +670,13 @@
     loop(1, S, lambda k: part_copy(k).wait_send())
     loop(1, T, lambda k: mod_copy(k).wait_send())
     loop(1, S, lambda k: ctx_copy(k).wait_send())
-    loop(1, T, lambda k: give(lax.rem(tp + k, T)).wait_send())
+    for r in range(Z):
+        for i in range(CORES):
+
+            @pl.when((r > 0) | (core != i))
+            def _():
+                give(r, i).wait_send()
+
     for i in range(3):
         own_mate(i).wait_send()
         w_lines[i].drain()
@@ -653,34 +717,31 @@
     QR, KR = down_q.shape[1], down_kv.shape[1]
     H = up_key.shape[1] // NOPE
 
-    def row(v):
-        return jnp.pad(v.astype(f32), (0, width - v.shape[0]))[None, :]
-
-    vectors = jnp.concatenate(
-        [row(v) for v in (cond, cond_context, norm_gain, qlat_gain, kvlat_gain)] + [jnp.zeros((3, width), f32)], axis=0
-    )
-    gain_q = jnp.broadcast_to(query_gain[:, None], (KD, 128))
-    gain_k = jnp.broadcast_to(key_gain[:, None], (KD, 128))
-    shift = (context_bias + math.log(TOK_DEV / CTX_DEV)) * math.log2(math.e)
-    shift = jnp.broadcast_to(shift[:, None], (H, 128))
+    def lines(v):
+        return v.reshape(-1, 128)
+
     tables = jnp.asarray(axial_tables(S * N))
-    args = (
-        vectors, gain_q, gain_k, shift, latent, context, mod_weight, dq, dkv, ow, rope_weight,
-        up_query, up_key, up_value, tables,
-    )
-    lat_rows, kv_rows = own_rows + 16, H * WIDE
+    small = [lines(v) for v in (cond, cond_context, norm_gain, qlat_gain, kvlat_gain)]
+    small += [query_gain[None, :], key_gain[None, :], context_bias[None, :]]
+    args = small + [
+        latent, context, mod_weight, dq, dkv, ow, rope_weight.T, up_query.T, up_key, up_value, tables,
+    ]
+    lat_rows, span = own_rows + 16, own_rows * CORES
     V = pltpu.VMEM
-    scratch = [
-        V(latent.shape, bf16), V(context.shape, bf16), V(mod_weight.shape, bf16), V(rope_weight.shape, bf16),
-        V(up_query.shape, bf16), V(up_key.shape, bf16), V(up_value.shape, bf16), V(tables.shape, f32),
-        V(up_query.shape[::-1], bf16), V((H * (NOPE + VDIM), KR), bf16),
+    scratch = [V(v.shape, v.dtype) for v in small[:5]]
+    scratch += [
+        V((2, 1, KD), f32), V((1, H), f32),
+        V(latent.shape, bf16), V(context.shape, bf16), V(mod_weight.shape, bf16), V(rope_weight.shape[::-1], bf16),
+        V(up_query.shape[::-1], bf16), V(up_key.shape, bf16), V(up_value.shape, bf16), V(tables.shape, f32),
+        V(up_key.shape[::-1], bf16), V((2, KD, 128), f32),
         V((Z, CORES) + dq.shape, bf16), V((Z, CORES) + dkv.shape, bf16), V((Z, CORES) + ow.shape, bf16),
         V((S, 8, cols), f32), V((8, cols), f32), V((T, 8, cols), f32), V((own_rows + ctx_rows, width), bf16),
         V((S, Z, CORES, lat_rows, KR), bf16), V((Z, CORES, own_rows, QR), bf16), V((S, ctx_rows + 16, KR), bf16),
-        V((H, N, 128), bf16), V((S, kv_rows, N), bf16), V((kv_rows, S * ctx_rows), bf16),
-        V((H, N, 128), f32), V((H, N, 128), f32), V((H, N, VDIM), f32),
+        V((H, N, 128), bf16), V((Z, H, KD, S * span), bf16), V((Z, H, S * span, 128), bf16),
+        V((H, KD, S * ctx_rows), bf16), V((H, S * ctx_rows, 128), bf16),
+        V((H, N, 128), f32), V((H, N, 128), f32),
         V((N, H * VDIM), bf16), V((T, own_rows, H * VDIM), bf16),
-        DMA((11,)), DMA((S,)), DMA((S,)), DMA((T,)), DMA((T,)),
+        DMA((19,)), DMA((S,)), DMA((S,)), DMA((T,)), DMA((T,)),
         DMA((3, Z, 2)), DMA((3, Z)), DMA((3, Z, S - 1)), DMA((3, Z, S)), DMA((3, Z)), DMA((3, Z)),
         DMA((2, Z, 2)), DMA((2, Z)), DMA((Z, S - 1)), DMA((Z, S)), DMA((S, Z)), DMA((S, Z)), DMA((Z,)), DMA((Z,)),
         DMA((S,)), DMA((S,)), DMA((T,)), DMA((T,)),
@@ -688,7 +749,7 @@
     return pl.pallas_call(
         kernel,
         out_shape=jax.ShapeDtypeStruct(latent.shape, bf16),
-        in_specs=[VM] * 4 + [ANY] * 11,
+        in_specs=[ANY] * len(args),
         out_specs=VM,
         scratch_shapes=scratch,
         compiler_params=pltpu.CompilerParams(

time: 115 us -> 93.5 us (0.81)
  Pallas kernels: 103 us -> 91.1 us
  local copies, waits for them, and re-layouts: 7.23 us -> 1.88 us
  other arithmetic: 4.13 us -> 0 us
    pallas_call x1, Pallas kernels: 103 us -> 91.1 us  [shards(): pl.pallas_call(kernel, out_shape=jax.ShapeDtypeStruct(latent.shape, bf16)...]
    broadcast_in_dim x5 -> x0, other arithmetic: 3.43 us -> none  [row(): return jnp.pad(v.astype(f32), (0, width - v.shape[0]))[None, :]]
    broadcast_in_dim x4 -> x0, local copies, waits for them, and re-layouts: 2.71 us -> none  [the longest x1 1.35 us: shards(): gain_q = jnp.broadcast_to(query_gain[:, None], (KD, 128))]
    unnamed x9 -> x1, local copies, waits for them, and re-layouts: 3.81 us -> 1.88 us
where the time goes in v2:
time: 93.5 us; the launch traced here: 93 us
  Pallas kernels  91.1 us (97%)
  local copies, waits for them, and re-layouts  1.88 us (2%)
    pallas_call x1, Pallas kernels, shards(): pl.pallas_call(kernel, out_shape=jax.ShapeDtypeStruct(latent.shape, bf16)...  91.1 us
    unnamed x1, local copies, waits for them, and re-layouts  1.88 us

profile of v2, /device:TPU:0, one launch (start us, length us, event | category | flops | bytes accessed | tf_op | source)
XLA Modules:
  0.0 93.0 jit_solution(13800971940251591333)
XLA Ops:
  0.0 91.1 %shard_map.181 = bf16[128,2048]{1,0:T(8,128)(2,1)} custom-call(bf16[16,128]{1,0:T(8,128)(2,1)} %bitcast.18, bf16[16,128]{1,0:T(8,128)(2,1)} %bitcast.19, bf16[16,128]{1,0:T(8,128)(2,1)} %bitcast.20, bf16[6,128]{1,0:T(8,128)(2,1)} %bitcast.21, bf16[4,128]{1,0:T(4,128)(2,1)} %bitcast.22, f32[1,96]{1,0:T(1,128)} %bitcast.23, f32[1,96]{1,0:T(1,128)} %bitcast.24, ...), custom_call_target="tpu_custom_call" | custom-call | tf_op jit(solution)/shard_map/pallas_call | solution.py:749
  91.1 1.9 %copy.21 = bf16[128,2048]{1,0:T(8,128)(2,1)} copy(bf16[128,2048]{1,0:T(8,128)(2,1)} %shard_map.181) | data formatting | bytes 1048576
